TPU v7x, 32 devices: a whole 2x2x4 slice. The times are simulated.
32 devices in a mesh: sp: 4 (over z), fs: 4 (over y, x), tp: 2 (over core).
Axes of the slice: x: 2, y: 2, z: 4, core: 2. Of those that a mesh axis runs over, the one named last changes fastest.
Arguments:
- tokens: bfloat16 [8, 1536, 2048], P('fs', ('sp', 'tp')), may hold values from -6 to 6
- norm_gain: float32 [2048], replicated, may hold values from 0.1 to 1.9
- chain_entry: bfloat16 [2048, 2048], P(('sp', 'fs'), 'tp'), may hold values from -0.125 to 0.125
- pool_entry: bfloat16 [2048, 2048], P(('sp', 'fs'), 'tp'), may hold values from -0.125 to 0.125
- conv_taps: bfloat16 [4, 2048], P(None, 'tp'), may hold values from -3 to 3
- recur_gate: bfloat16 [8, 256, 256], P('tp'), may hold values from -0.375 to 0.375
- input_gate: bfloat16 [8, 256, 256], P('tp'), may hold values from -0.375 to 0.375
- decay_log: float32 [2048], P('tp'), may hold values from -9 to 5
- decay_shift: float32 [8, 1536, 2048], P('fs', 'sp', 'tp'), may hold values from -1 to 0
- start_state: float32 [8, 2048], P('fs', 'tp'), may hold values from -6 to 6
- pool_mix: bfloat16 [8, 256, 256], P('tp'), may hold values from -0.375 to 0.375
- pool_scale: float32 [2048], P('tp'), may hold values from 0.1 to 1.9
- chain_exit: bfloat16 [2048, 2048], P('tp', ('sp', 'fs')), may hold values from -0.09375 to 0.09375
- pool_exit: bfloat16 [2048, 2048], P('tp', ('sp', 'fs')), may hold values from -0.09375 to 0.09375
Outputs:
- mixed_rows: bfloat16 [8, 1536, 2048], P('fs', ('sp', 'tp'))
All inputs are finite; a program needn't handle non-finite values.
Results may differ from a plain program's by a relative error of at most 0.01.
Values may be sent and summed in bfloat16 or wider, within the bound.
No kernel may reach another device: no remote copies, remote signals or barrier semaphores. Data moves between devices by JAX's collectives and lax.ppermute only.
A program may use at most 128 MiB of HBM per device.

v0:
```python
import functools

import jax
import jax.numpy as jnp
from jax import lax
from jax.experimental import pallas as pl
from jax.experimental.pallas import tpu as pltpu
from jax.sharding import PartitionSpec as P


HALO = 16
LANES = 128
NORM_EPSILON = 1e-06
RECUR_SCALE = 8.0
CHUNKS = 8
MIB = 1024 * 1024
ROUTES = {"E1": ("xy", "yx", "xy", "yx"), "E2": ("xy", "yx", "xy", "yx"), "X1": "yzx", "X2": "xzy"}
LATE_LAPS = 1


def ring_pairs(size):
    return [(i, (i + 1) % size) for i in range(size)]


def swap_pairs(size, bit):
    return [(i, i ^ bit) for i in range(size)]


def join(values):
    return jnp.concatenate(values, axis=0)


def gather_part(own, route, sp_n, fs_n):
    own = own[None]
    ring = ring_pairs(sp_n)

    def swapped(part, step):
        stack, places = part
        bit = 1 if step == "x" else 2
        came = lax.ppermute(stack, "fs", swap_pairs(fs_n, bit))
        return came, [(f ^ bit, s) for f, s in places]

    found = []
    if isinstance(route, tuple):
        held = (own, [(0, 0)])
        for lap in range(sp_n):
            if lap:
                held = (lax.ppermute(held[0], "sp", ring), [(0, lap)])
            one, two = route[lap % len(route)]
            first = swapped(held, one)
            found += [held, first]
            found += [swapped(held, two), swapped(first, two)]
    elif route[0] == "z":
        one, two = route[1], route[2]
        laps = [own]
        for _ in range(1, sp_n):
            laps.append(lax.ppermute(laps[-1], "sp", ring))
        for group in (range(0, sp_n // 2), range(sp_n // 2, sp_n)):
            held = join([laps[i] for i in group])
            held = (held, [(0, i) for i in group])
            first = swapped(held, one)
            found += [held, first]
            found += [swapped(held, two), swapped(first, two)]
    else:
        one, two = route[0], route[2]
        first = swapped((own, [(0, 0)]), one)
        held = (join([own, first[0]]), [(0, 0)] + first[1])
        for lap in range(sp_n):
            if lap:
                stack = lax.ppermute(held[0], "sp", ring)
                held = (stack, [(f, lap) for f, _ in held[1]])
            found += [held, swapped(held, two)]
    return [(stack, [f * sp_n + s for f, s in places]) for stack, places in found]


def norm_kernel(order, side, own, other, halo, gain, out):
    blocks = own.shape[2] // LANES
    half = own.shape[1]
    width = own.shape[2]

    def rows_of(src, base, count, size):
        def one(i, _):
            at = pl.multiple_of(i * size, size)
            squares = None
            for b in range(blocks):
                part = src[0, pl.ds(at, size), b * LANES : (b + 1) * LANES].astype(jnp.float32)
                squares = part * part if squares is None else squares + part * part
            mean = jnp.sum(squares, axis=-1, keepdims=True) * (1.0 / width)
            scale = jnp.broadcast_to(lax.rsqrt(mean + NORM_EPSILON), (size, LANES))
            to = pl.multiple_of(base + i * size, HALO)
            for b in range(blocks):
                col = pl.multiple_of(order[b] * LANES, LANES)
                part = src[0, pl.ds(at, size), pl.ds(col, LANES)].astype(jnp.float32)
                out[0, pl.ds(to, size), b * LANES : (b + 1) * LANES] = (
                    part * scale * gain[:, pl.ds(col, LANES)]
                ).astype(out.dtype)
            return 0

        lax.fori_loop(0, count, one, 0)

    size = 64 if half % 64 == 0 else HALO
    rows_of(halo, 0, 1, HALO)
    rows_of(own, HALO + side[0] * half, half // size, size)
    rows_of(other, HALO + (1 - side[0]) * half, half // size, size)


def norm_rows(order, side, own, other, halo, gain):
    seqs, half, width = own.shape
    rows = 2 * half + HALO
    return pl.pallas_call(
        norm_kernel,
        out_shape=jax.ShapeDtypeStruct((seqs, rows, width), jnp.bfloat16),
        grid_spec=pltpu.PrefetchScalarGridSpec(
            num_scalar_prefetch=2,
            grid=(seqs,),
            in_specs=[
                pl.BlockSpec((1, half, width), lambda i, *_: (i, 0, 0)),
                pl.BlockSpec((1, half, width), lambda i, *_: (i, 0, 0)),
                pl.BlockSpec((1, HALO, width), lambda i, *_: (i, 0, 0)),
                pl.BlockSpec((1, width), lambda i, *_: (0, 0)),
            ],
            out_specs=pl.BlockSpec((1, rows, width), lambda i, *_: (i, 0, 0)),
        ),
        compiler_params=pltpu.CompilerParams(vmem_limit_bytes=24 * MIB),
        cost_estimate=pl.CostEstimate(flops=4_000_000_000, transcendentals=0, bytes_accessed=8_000_000),
        name="norm_rows",
    )(order, side, own, other, halo, gain.reshape(1, width))


def entry_kernel(places, seqs, x, *refs):
    stacks, (out, held, sems) = refs[: len(places)], refs[len(places) :]
    depth = stacks[0].shape[1]
    tiles, _, tile = held.shape
    rows = x.shape[0] // seqs

    def copies(j):
        return [
            pltpu.make_async_copy(
                stack.at[m, :, pl.ds(j * tile, tile)],
                held.at[j, pl.ds(r * depth, depth), :],
                sems.at[j, r],
            )
            for stack, places_of in zip(stacks, places)
            for m, r in enumerate(places_of)
        ]

    for j in range(tiles):
        for copy in copies(j):
            copy.start()
    for j in range(tiles):
        for copy in copies(j):
            copy.wait()
        for s in range(seqs):
            out[s * rows : (s + 1) * rows, j * tile : (j + 1) * tile] = jnp.dot(
                x[s * rows : (s + 1) * rows, :], held[j], preferred_element_type=jnp.float32
            ).astype(out.dtype)


def entry_dot(x, parts):
    seqs, total, depth = x.shape
    rows = seqs * total
    width = parts[0][0].shape[2]
    tile = min(2 * LANES, width)
    shards = depth // parts[0][0].shape[1]
    return pl.pallas_call(
        functools.partial(entry_kernel, [places for _, places in parts], seqs),
        out_shape=jax.ShapeDtypeStruct((rows, width), jnp.bfloat16),
        in_specs=[pl.BlockSpec(memory_space=pltpu.VMEM)]
        + [pl.BlockSpec(memory_space=pl.ANY)] * len(parts),
        out_specs=pl.BlockSpec(memory_space=pltpu.VMEM),
        scratch_shapes=[
            pltpu.VMEM((width // tile, depth, tile), jnp.bfloat16),
            pltpu.SemaphoreType.DMA((width // tile, shards)),
        ],
        compiler_params=pltpu.CompilerParams(vmem_limit_bytes=20 * MIB),
        cost_estimate=pl.CostEstimate(
            flops=2 * rows * depth * width, transcendentals=0, bytes_accessed=2 * depth * width
        ),
    )(x.reshape(rows, depth), *[stack for stack, _ in parts]).reshape(seqs, total, width)


def chain_kernel(length, x, taps, wr, wi, rate_log, shift, h_out, p_out, seam_h, seam_p, wide):
    rows = shift.shape[1]
    span = rows // CHUNKS
    tap_count = taps.shape[0]
    wide[...] = x[0].astype(jnp.float32)
    first = HALO - (tap_count - 1)
    conv = wide[first : first + rows, :] * taps[0:1, :].astype(jnp.float32)
    for j in range(1, tap_count):
        conv = conv + wide[first + j : first + j + rows, :] * taps[j : j + 1, :].astype(jnp.float32)
    conv = conv.astype(jnp.bfloat16)
    to_recur = jnp.dot(conv, wr[0], preferred_element_type=jnp.float32)
    to_input = jnp.dot(conv, wi[0], preferred_element_type=jnp.float32)
    gate_recur = 0.5 * jnp.tanh(0.5 * to_recur) + 0.5
    gate_input = 0.5 * jnp.tanh(0.5 * to_input) + 0.5
    rate = jnp.exp(rate_log[...]) * (-RECUR_SCALE / length)
    log_decay = gate_recur * rate + shift[0]
    decay = jnp.exp(log_decay)
    twice = 2.0 * log_decay
    series = 1.0 + twice * (1.0 / 8.0)
    for k in range(7, 1, -1):
        series = 1.0 + twice * (1.0 / k) * series
    gone = jnp.where(twice > -0.5, -twice * series, 1.0 - decay * decay)
    root = gone * lax.rsqrt(jnp.maximum(gone, 1e-37))
    drive = root * gate_input * conv.astype(jnp.float32)
    width = wide.shape[1]
    lanes = [slice(b * LANES, (b + 1) * LANES) for b in range(width // LANES)]
    for b, cols in enumerate(lanes):
        p_out[0, b] = decay[:, cols]
        h_out[0, b] = drive[:, cols]
    states = [jnp.zeros((CHUNKS, LANES), jnp.float32) for _ in lanes]
    keeps = [jnp.ones((CHUNKS, LANES), jnp.float32) for _ in lanes]
    for t in range(span):
        step = pl.ds(t, CHUNKS, stride=span)
        for b in range(len(lanes)):
            a = p_out[0, b, step, :]
            states[b] = a * states[b] + h_out[0, b, step, :]
            keeps[b] = a * keeps[b]
            h_out[0, b, step, :] = states[b]
            p_out[0, b, step, :] = keeps[b]
    state = jnp.concatenate(states, axis=1)
    kept = jnp.concatenate(keeps, axis=1)
    before_h = jnp.zeros((1, width), jnp.float32)
    before_p = jnp.ones((1, width), jnp.float32)
    for c in range(CHUNKS):
        seam_h[0, c : c + 1, :] = before_h
        seam_p[0, c : c + 1, :] = before_p
        before_h = kept[c : c + 1] * before_h + state[c : c + 1]
        before_p = kept[c : c + 1] * before_p
    seam_h[0, CHUNKS : 2 * CHUNKS, :] = jnp.broadcast_to(before_h, (CHUNKS, width))
    seam_p[0, CHUNKS : 2 * CHUNKS, :] = jnp.broadcast_to(before_p, (CHUNKS, width))


def chain_scan(x, taps, wr, wi, rate_log, shift, length):
    seqs, rows, width = shift.shape
    heads, head, _ = wr.shape
    return pl.pallas_call(
        functools.partial(chain_kernel, length),
        out_shape=(
            jax.ShapeDtypeStruct((seqs, width // LANES, rows, LANES), jnp.float32),
            jax.ShapeDtypeStruct((seqs, width // LANES, rows, LANES), jnp.float32),
            jax.ShapeDtypeStruct((seqs, 2 * CHUNKS, width), jnp.float32),
            jax.ShapeDtypeStruct((seqs, 2 * CHUNKS, width), jnp.float32),
        ),
        grid=(seqs, heads),
        in_specs=[
            pl.BlockSpec((1, rows + HALO, head), lambda i, g: (i, 0, g)),
            pl.BlockSpec((taps.shape[0], head), lambda i, g: (0, g)),
            pl.BlockSpec((1, head, head), lambda i, g: (g, 0, 0)),
            pl.BlockSpec((1, head, head), lambda i, g: (g, 0, 0)),
            pl.BlockSpec((1, head), lambda i, g: (0, g)),
            pl.BlockSpec((1, rows, head), lambda i, g: (i, 0, g)),
        ],
        out_specs=(
            pl.BlockSpec((1, head // LANES, rows, LANES), lambda i, g: (i, g, 0, 0)),
            pl.BlockSpec((1, head // LANES, rows, LANES), lambda i, g: (i, g, 0, 0)),
            pl.BlockSpec((1, 2 * CHUNKS, head), lambda i, g: (i, 0, g)),
            pl.BlockSpec((1, 2 * CHUNKS, head), lambda i, g: (i, 0, g)),
        ),
        scratch_shapes=[pltpu.VMEM((rows + HALO, head), jnp.float32)],
        compiler_params=pltpu.CompilerParams(vmem_limit_bytes=24 * MIB),
        cost_estimate=pl.CostEstimate(
            flops=8_000_000_000, transcendentals=0, bytes_accessed=12_000_000
        ),
        name="chain_scan",
    )(x, taps, wr, wi, rate_log.reshape(1, width), shift)


def pool_kernel(start, x, mix, scale, out, wide, sums):
    rows = out.shape[1]
    total = rows + HALO
    low, high = 8, 8 + total
    first = low + HALO
    group = lax.rem(pl.program_id(1), 4)
    width = wide.shape[1]
    wide[0:low, :] = jnp.zeros((low, width), jnp.float32)
    wide[low:high, :] = x[0].astype(jnp.float32)

    def finish(trail, window):
        place = start[0] + lax.broadcasted_iota(jnp.int32, (rows, LANES), 0)
        counts = jnp.minimum(place.astype(jnp.float32) + 1.0, window)
        inverse = jnp.concatenate([1.0 / counts] * (width // LANES), axis=1)
        diff = (trail * inverse - wide[first:high, :]).astype(jnp.bfloat16)
        mapped = jnp.dot(diff, mix[0], preferred_element_type=jnp.float32)
        out[0] = (mapped * scale[...]).astype(out.dtype)

    for depth in range(4):

        @pl.when(group == depth)
        def _(depth=depth):
            held = wide
            for level in range(depth):
                reach = 2**level
                sums[level, 0:low, :] = jnp.zeros((low, width), jnp.float32)
                sums[level, low:high, :] = held[low:high, :] + held[low - reach : high - reach, :]
                held = sums.at[level]
            reach = 2**depth
            finish(held[first:high, :] + held[first - reach : high - reach, :], 2.0 * reach)


def pool_mixed(start, x, mix, scale):
    seqs, total, width = x.shape
    groups, head, _ = mix.shape
    assert groups % 4 == 0
    rows = total - HALO
    return pl.pallas_call(
        pool_kernel,
        out_shape=jax.ShapeDtypeStruct((seqs, rows, width), jnp.bfloat16),
        grid_spec=pltpu.PrefetchScalarGridSpec(
            num_scalar_prefetch=1,
            grid=(seqs, groups),
            in_specs=[
                pl.BlockSpec((1, total, head), lambda i, g, *_: (i, 0, g)),
                pl.BlockSpec((1, head, head), lambda i, g, *_: (g, 0, 0)),
                pl.BlockSpec((1, head), lambda i, g, *_: (0, g)),
            ],
            out_specs=pl.BlockSpec((1, rows, head), lambda i, g, *_: (i, 0, g)),
            scratch_shapes=[
                pltpu.VMEM((8 + total, head), jnp.float32),
                pltpu.VMEM((3, 8 + total, head), jnp.float32),
            ],
        ),
        compiler_params=pltpu.CompilerParams(vmem_limit_bytes=24 * MIB),
        cost_estimate=pl.CostEstimate(
            flops=4_000_000_000, transcendentals=0, bytes_accessed=4_000_000
        ),
        name="pool_mixed",
    )(start, x, mix, scale.reshape(1, width))


def recurrent_kernel(h, p, seam_h, seam_p, entering, out):
    seqs, blocks, rows, _ = h.shape
    span = rows // CHUNKS
    for s in range(seqs):
        for b in range(blocks):
            cols = slice(b * LANES, (b + 1) * LANES)
            for c in range(CHUNKS):
                one = slice(c, c + 1)
                gone_in = seam_h[s, one, cols] + seam_p[s, one, cols] * entering[s : s + 1, cols]
                at = slice(c * span, (c + 1) * span)
                out[s, at, cols] = (h[s, b, at, :] + p[s, b, at, :] * gone_in).astype(out.dtype)


def recurrent_rows(h, p, seam_h, seam_p, entering):
    seqs, blocks, rows, _ = h.shape
    vmem = pl.BlockSpec(memory_space=pltpu.VMEM)
    return pl.pallas_call(
        recurrent_kernel,
        out_shape=jax.ShapeDtypeStruct((seqs, rows, blocks * LANES), jnp.bfloat16),
        in_specs=[vmem] * 5,
        out_specs=vmem,
        compiler_params=pltpu.CompilerParams(vmem_limit_bytes=16 * MIB),
        cost_estimate=pl.CostEstimate(
            flops=2_000_000_000, transcendentals=0, bytes_accessed=8_000_000
        ),
    )(h, p, seam_h, seam_p, entering)


def exit_kernel(chain_spots, pool_spots, counts, shards, merged, *refs):
    if merged:
        order, side, recurrent, pooled, came, *refs = refs
    else:
        side, recurrent, pooled, *refs = refs
    chain_stacks, pool_stacks = refs[: counts[0]], refs[counts[0] : sum(counts)]
    refs = refs[sum(counts) :]
    if merged:
        out, held, sem = refs[-3:]
    else:
        (out,) = refs
    seqs, rows, _ = recurrent.shape
    half = rows // 2
    at = pl.ds(pl.multiple_of(side[0] * half, half), half)
    left = jnp.concatenate([recurrent[s, at, :] for s in range(seqs)], axis=0)
    left_pool = jnp.concatenate([pooled[s, at, :] for s in range(seqs)], axis=0)

    def columns(stacks, spots, pair):
        found = []
        for i in pair:
            stack, m = spots[shards[i]]
            found.append(stacks[stack][m])
        return jnp.concatenate(found, axis=1)

    copies = []
    for j in range(0, len(shards), 2):
        pair = range(j, min(j + 2, len(shards)))
        got = jnp.dot(
            left, columns(chain_stacks, chain_spots, pair), preferred_element_type=jnp.float32
        ) + jnp.dot(
            left_pool, columns(pool_stacks, pool_spots, pair), preferred_element_type=jnp.float32
        )
        cols = slice(j * LANES, (j + len(pair)) * LANES)
        for s in range(seqs):
            rows_of = got[s * half : (s + 1) * half]
            if merged:
                rows_of = rows_of + came[s, :, cols].astype(jnp.float32)
                held[s, :, cols] = rows_of.astype(out.dtype)
            else:
                out[s, :, cols] = rows_of.astype(out.dtype)
        if merged:
            for i in pair:
                to = pl.multiple_of(order[shards[i]] * LANES, LANES)
                copies.append(
                    pltpu.make_async_copy(
                        held.at[:, :, i * LANES : (i + 1) * LANES],
                        out.at[:, :, pl.ds(to, LANES)],
                        sem.at[i],
                    )
                )
                copies[-1].start()
    for copy in copies:
        copy.wait()


def exit_columns(side, recurrent, pooled, chain_parts, pool_parts, shards, merge=None):
    seqs, rows, width = recurrent.shape
    half = rows // 2
    wide = len(shards) * LANES

    def used(parts):
        kept = [q for q in parts if any(r in shards for r in q[1])]
        return [q[0] for q in kept], {r: (i, m) for i, q in enumerate(kept) for m, r in enumerate(q[1])}

    chain_stacks, chain_spots = used(chain_parts)
    pool_stacks, pool_spots = used(pool_parts)
    counts = (len(chain_stacks), len(pool_stacks))
    vmem = pl.BlockSpec(memory_space=pltpu.VMEM)
    smem = pl.BlockSpec(memory_space=pltpu.SMEM)
    stacks = (*chain_stacks, *pool_stacks)
    if merge is None:
        args = (side, recurrent, pooled, *stacks)
        specs = [smem] + [vmem] * (len(args) - 1)
        out_shape = jax.ShapeDtypeStruct((seqs, half, wide), jnp.bfloat16)
        extra = dict(out_specs=vmem)
    else:
        order, came, result = merge
        args = (order, side, recurrent, pooled, came, *stacks)
        specs = [smem, smem] + [vmem] * (len(args) - 2)
        aliases = {}
        if result is not None:
            args, specs = (*args, result), specs + [pl.BlockSpec(memory_space=pl.ANY)]
            aliases = {len(args) - 1: 0}
        out_shape = jax.ShapeDtypeStruct((seqs, half, order.shape[0] * LANES), jnp.bfloat16)
        extra = dict(
            out_specs=pl.BlockSpec(memory_space=pl.ANY),
            input_output_aliases=aliases,
            scratch_shapes=[
                pltpu.VMEM((seqs, half, wide), jnp.bfloat16),
                pltpu.SemaphoreType.DMA((len(shards),)),
            ],
        )
    return pl.pallas_call(
        functools.partial(exit_kernel, chain_spots, pool_spots, counts, shards, merge is not None),
        out_shape=out_shape,
        in_specs=specs,
        compiler_params=pltpu.CompilerParams(vmem_limit_bytes=32 * MIB),
        cost_estimate=pl.CostEstimate(
            flops=4 * seqs * half * width * wide, transcendentals=0, bytes_accessed=6_000_000
        ),
        **extra,
    )(*args)


def weights_and_order(chain_entry, pool_entry, chain_exit, pool_exit, width):
    sp_n, fs_n = lax.axis_size("sp"), lax.axis_size("fs")
    if chain_entry.shape[0] % LANES == 0 and chain_exit.shape[1] == LANES and fs_n == 4:
        go = lambda own, name: gather_part(own, ROUTES[name], sp_n, fs_n)
        found = go(chain_entry, "E1"), go(pool_entry, "E2"), go(chain_exit, "X1"), go(pool_exit, "X2")
        place, spot = lax.axis_index("sp"), lax.axis_index("fs")
        lap = jnp.arange(sp_n, dtype=jnp.int32)[None, :]
        swap = jnp.arange(fs_n, dtype=jnp.int32)[:, None]
        order = ((place - lap) % sp_n) * fs_n + (spot ^ swap)
        return found, order.reshape(-1).astype(jnp.int32)
    blocks = width // LANES
    places = list(range(blocks))
    entry = lambda w: [
        (lax.all_gather(w, ("sp", "fs"), axis=0, tiled=True).reshape(blocks, -1, w.shape[1]), places)
    ]
    leave = lambda w: [
        (
            lax.all_gather(w, ("sp", "fs"), axis=1, tiled=True)
            .reshape(w.shape[0], blocks, LANES)
            .transpose(1, 0, 2),
            places,
        )
    ]
    found = entry(chain_entry), entry(pool_entry), leave(chain_exit), leave(pool_exit)
    return found, jnp.arange(blocks, dtype=jnp.int32)


def per_device(
    tokens,
    norm_gain,
    chain_entry,
    pool_entry,
    conv_taps,
    recur_gate,
    input_gate,
    decay_log,
    decay_shift,
    start_state,
    pool_mix,
    pool_scale,
    chain_exit,
    pool_exit,
):
    sp_n, tp_n = lax.axis_size("sp"), lax.axis_size("tp")
    assert tp_n == 2
    _, half, width = tokens.shape
    rows = half * tp_n
    place, core = lax.axis_index("sp"), lax.axis_index("tp")
    side = jnp.reshape(core, (1,)).astype(jnp.int32)
    other_side = 1 - side
    (ce, pe, cx, px), order = weights_and_order(chain_entry, pool_entry, chain_exit, pool_exit, width)

    swap_tp = [(0, 1), (1, 0)]
    other = lax.ppermute(tokens, "tp", swap_tp)
    tail = jnp.where(core == 1, tokens[:, half - HALO :], other[:, half - HALO :])
    halo = lax.ppermute(tail, "sp", [(i, i + 1) for i in range(sp_n - 1)])
    normed = norm_rows(order, side, tokens, other, halo, norm_gain)

    chain_input = entry_dot(normed, ce)
    pool_input = entry_dot(normed, pe)

    h, p, seam_h, seam_p = chain_scan(
        chain_input, conv_taps, recur_gate, input_gate, decay_log, decay_shift, rows * sp_n
    )
    last = jnp.stack([seam_p[:, CHUNKS], seam_h[:, CHUNKS]])
    entering = start_state
    for back in range(sp_n - 1, 0, -1):
        came = lax.ppermute(last, "sp", [(i, i + back) for i in range(sp_n - back)])
        entering = jnp.where(place >= back, came[0] * entering + came[1], entering)

    start = jnp.reshape(place * rows, (1,)).astype(jnp.int32)
    pooled = pool_mixed(start, pool_input, pool_mix, pool_scale)

    recurrent = recurrent_rows(h, p, seam_h, seam_p, entering)

    count = order.shape[0]
    laps = sp_n if count % sp_n == 0 else count
    late = tuple(r for r in range(count) if r % laps >= laps - LATE_LAPS)
    early = tuple(r for r in range(count) if r % laps < laps - LATE_LAPS)
    ex = lambda at, shards, merge=None: exit_columns(at, recurrent, pooled, cx, px, shards, merge)
    came_early = lax.ppermute(ex(other_side, early), "tp", swap_tp)
    came_late = lax.ppermute(ex(other_side, late), "tp", swap_tp)
    result = ex(side, early, (order, came_early, None))
    return ex(side, late, (order, came_late, result))


def solution(mesh):
    in_specs = (
        P("fs", ("sp", "tp"), None),
        P(),
        P(("sp", "fs"), "tp"),
        P(("sp", "fs"), "tp"),
        P(None, "tp"),
        P("tp", None, None),
        P("tp", None, None),
        P("tp"),
        P("fs", "sp", "tp"),
        P("fs", "tp"),
        P("tp", None, None),
        P("tp"),
        P("tp", ("sp", "fs")),
        P("tp", ("sp", "fs")),
    )
    out_specs = P("fs", ("sp", "tp"), None)

    return jax.shard_map(per_device, mesh=mesh, in_specs=in_specs, out_specs=out_specs, check_vma=False)
```

profile of v0, /device:TPU:1, one launch (start us, length us, event | category | flops | bytes accessed | tf_op | source)
XLA Modules:
  0.0 170.4 jit_solution(11654244677039497777)
XLA Ops:
  0.0 2.8 %collective-permute-start.5 = (bf16[1,128,1024]{2,1,0:T(8,128)(2,1)}, bf16[1,128,1024]{2,1,0:T(8,128)(2,1)}, u32[]{:S(2)}, u32[]{:S(2)}) collective-permute-start(bf16[1,128,1024]{2,1,0:T(8,128)(2,1)} %bitcast.64), channel_id=1, source_target_pairs={{0,8},{8,16},{16,24},{24,0},{1,9},{9,17},{17,25},{25,1},{2,10},{10... | collective-permute-start | bytes 786440 | tf_op jit(solution)/shard_map/ppermute | solution.py:48
  2.8 1.2 collective-permute-start.2
  4.0 1.2 collective-permute-start.3
  5.2 1.3 collective-permute-start.23
  6.5 5.2 %collective-permute-done.5.refs_4_ = bf16[1,128,1024]{2,1,0:T(8,128)(2,1)} collective-permute-done((bf16[1,128,1024]{2,1,0:T(8,128)(2,1)}, bf16[1,128,1024]{2,1,0:T(8,128)(2,1)}, u32[]{:S(2)}, u32[]{:S(2)}) %collective-permute-start.5) | collective-permute-done | bytes 262176 | tf_op jit(solution)/shard_map/ppermute | solution.py:48
  11.8 1.0 collective-permute-start.20
  12.8 1.2 collective-permute-start.21
  14.9 2.3 %collective-permute-done.23.refs_4_ = bf16[1,128,1024]{2,1,0:T(8,128)(2,1)S(1)} collective-permute-done((bf16[1,128,1024]{2,1,0:T(8,128)(2,1)}, bf16[1,128,1024]{2,1,0:T(8,128)(2,1)S(1)}, u32[]{:S(2)}, u32[]{:S(2)}) %collective-permute-start.23) | collective-permute-done | bytes 262176 | tf_op jit(solution)/shard_map/ppermute | solution.py:48
  17.3 1.8 %collective-permute-done.20.refs_1_ = bf16[1,128,1024]{2,1,0:T(8,128)(2,1)} collective-permute-done((bf16[1,128,1024]{2,1,0:T(8,128)(2,1)}, bf16[1,128,1024]{2,1,0:T(8,128)(2,1)}, u32[]{:S(2)}, u32[]{:S(2)}) %collective-permute-start.20) | collective-permute-done | bytes 262176 | tf_op jit(solution)/shard_map/ppermute | solution.py:40
  19.6 1.2 collective-permute-start.6
  20.9 4.1 %collective-permute-done.35 = bf16[1,1024,128]{2,1,0:T(8,128)(2,1)} collective-permute-done((bf16[1,1024,128]{2,1,0:T(8,128)(2,1)}, bf16[1,1024,128]{2,1,0:T(8,128)(2,1)}, u32[]{:S(2)}, u32[]{:S(2)}) %collective-permute-start.35) | collective-permute-done | bytes 262176 | tf_op jit(solution)/shard_map/ppermute | solution.py:40
  27.2 3.4 %collective-permute-done.6.refs_5_ = bf16[1,128,1024]{2,1,0:T(8,128)(2,1)} collective-permute-done((bf16[1,128,1024]{2,1,0:T(8,128)(2,1)}, bf16[1,128,1024]{2,1,0:T(8,128)(2,1)}, u32[]{:S(2)}, u32[]{:S(2)}) %collective-permute-start.6) | collective-permute-done | bytes 262176 | tf_op jit(solution)/shard_map/ppermute | solution.py:40
  30.6 1.2 collective-permute-start.24
  32.1 1.9 %collective-permute-done.13.refs_12_ = bf16[1,128,1024]{2,1,0:T(8,128)(2,1)} collective-permute-done((bf16[1,128,1024]{2,1,0:T(8,128)(2,1)}, bf16[1,128,1024]{2,1,0:T(8,128)(2,1)}, u32[]{:S(2)}, u32[]{:S(2)}) %collective-permute-start.13) | collective-permute-done | bytes 262176 | tf_op jit(solution)/shard_map/ppermute | solution.py:48
  34.7 1.2 collective-permute-start.14
  36.9 4.7 %collective-permute-done.4.refs_3_ = bf16[1,128,1024]{2,1,0:T(8,128)(2,1)S(1)} collective-permute-done((bf16[1,128,1024]{2,1,0:T(8,128)(2,1)}, bf16[1,128,1024]{2,1,0:T(8,128)(2,1)S(1)}, u32[]{:S(2)}, u32[]{:S(2)}) %collective-permute-start.4) | collective-permute-done | bytes 262176 | tf_op jit(solution)/shard_map/ppermute | solution.py:40
  41.6 1.3 collective-permute-start.1
  42.9 1.1 pad_maximum_fusion.refs_3_.refs_5_
  44.0 1.1 pad_maximum_fusion.1.refs_9_.refs_11_
  45.1 1.3 collective-permute-start.11
  46.4 1.2 collective-permute-start.8
  48.5 0.9 collective-permute-start.16
  49.4 2.9 %norm_rows.1 = bf16[2,400,2048]{2,1,0:T(8,128)(2,1)S(1)} custom-call(s32[16]{0:T(128)S(1)} %add.41.order.refs_0_, s32[1]{0:T(128)} %bitcast.side.refs_1_, bf16[2,192,2048]{2,1,0:T(8,128)(2,1)S(1)} %copy-done, bf16[2,192,2048]{2,1,0:T(8,128)(2,1)S(1)} %collective-permute-done.other, bf16[2,16,2048]{2,1,0:T(8,128)(2,1)S(1)} %collective-permute-done.1.halo, ...), custom_call_target="tpu_custom_call" | custom-call | flops 4000000000 | bytes 8000000 | tf_op jit(solution)/shard_map/norm_rows/pallas_call | solution.py:110
  55.2 1.5 collective-permute-done.12.refs_11_
  57.0 2.2 %collective-permute-done.16.refs_15_ = bf16[1,128,1024]{2,1,0:T(8,128)(2,1)S(1)} collective-permute-done((bf16[1,128,1024]{2,1,0:T(8,128)(2,1)S(1)}, bf16[1,128,1024]{2,1,0:T(8,128)(2,1)S(1)}, u32[]{:S(2)}, u32[]{:S(2)}) %collective-permute-start.16) | collective-permute-done | bytes 262176 | tf_op jit(solution)/shard_map/ppermute | solution.py:40
  59.4 5.9 %shard_map.136 = bf16[800,1024]{1,0:T(8,128)(2,1)S(1)} custom-call(bf16[800,2048]{1,0:T(8,128)(2,1)S(1)} %bitcast.75, bf16[1,128,1024]{2,1,0:T(8,128)(2,1)S(1)} %bitcast.67, bf16[1,128,1024]{2,1,0:T(8,128)(2,1)} %collective-permute-done.2.refs_1_, bf16[1,128,1024]{2,1,0:T(8,128)(2,1)S(1)} %copy-done.8, ...), custom_call_target="tpu_custom_call" | custom-call | flops 3355443200 | bytes 4194304 | tf_op jit(solution)/shard_map/pallas_call | solution.py:165
  65.4 1.2 collective-permute-start.46
  67.6 2.8 %collective-permute-done.28.refs_9_ = bf16[1,128,1024]{2,1,0:T(8,128)(2,1)S(1)} collective-permute-done((bf16[1,128,1024]{2,1,0:T(8,128)(2,1)S(1)}, bf16[1,128,1024]{2,1,0:T(8,128)(2,1)S(1)}, u32[]{:S(2)}, u32[]{:S(2)}) %collective-permute-start.28) | collective-permute-done | bytes 262176 | tf_op jit(solution)/shard_map/ppermute | solution.py:40
  71.8 12.3 %chain_scan.1 = (f32[2,8,384,128]{3,2,1,0:T(8,128)S(1)}, f32[2,8,384,128]{3,2,1,0:T(8,128)S(1)}, f32[2,16,1024]{2,1,0:T(8,128)S(1)}, f32[2,16,1024]{2,1,0:T(8,128)S(1)}) custom-call(bf16[2,400,1024]{2,1,0:T(8,128)(2,1)S(1)} %bitcast.77, bf16[4,1024]{1,0:T(4,128)(2,1)S(1)} %copy-done.10, bf16[4,256,256]{2,1,0:T(8,128)(2,1)S(1)} %copy-done.2, ...), custom_call_target="tpu_custom_call" | custom-call | flops 8000000000 | bytes 12000000 | tf_op jit(solution)/shard_map/chain_scan/pallas_call | solution.py:237
  84.4 2.7 %collective-permute-done.26.refs_7_ = bf16[1,128,1024]{2,1,0:T(8,128)(2,1)S(1)} collective-permute-done((bf16[1,128,1024]{2,1,0:T(8,128)(2,1)S(1)}, bf16[1,128,1024]{2,1,0:T(8,128)(2,1)S(1)}, u32[]{:S(2)}, u32[]{:S(2)}) %collective-permute-start.26) | collective-permute-done | bytes 262176 | tf_op jit(solution)/shard_map/ppermute | solution.py:40
  88.5 1.0 collective-permute-start.42
  89.6 1.5 collective-permute-start.34
  91.1 4.3 %collective-permute-done.33.refs_14_ = bf16[1,128,1024]{2,1,0:T(8,128)(2,1)S(1)} collective-permute-done((bf16[1,128,1024]{2,1,0:T(8,128)(2,1)S(1)}, bf16[1,128,1024]{2,1,0:T(8,128)(2,1)S(1)}, u32[]{:S(2)}, u32[]{:S(2)}) %collective-permute-start.33) | collective-permute-done | bytes 262176 | tf_op jit(solution)/shard_map/ppermute | solution.py:40
  95.4 1.9 %collective-permute-start.17 = (f32[2,2,1024]{2,1,0:T(2,128)S(1)}, f32[2,2,1024]{2,1,0:T(2,128)S(1)}, u32[]{:S(2)}, u32[]{:S(2)}) collective-permute-start(f32[2,2,1024]{2,1,0:T(2,128)S(1)} %pad_maximum_fusion.2), channel_id=1, source_target_pairs={{0,8},{8,16},{16,24},{1,9},{9,17},{17,25},{2,10},{10,18},{18,26},{... | collective-permute-start | bytes 49160 | tf_op jit(solution)/shard_map/ppermute | solution.py:530
  97.3 4.0 %collective-permute-start.18 = (f32[2,2,1024]{2,1,0:T(2,128)S(1)}, f32[2,2,1024]{2,1,0:T(2,128)S(1)}, u32[]{:S(2)}, u32[]{:S(2)}) collective-permute-start(f32[2,2,1024]{2,1,0:T(2,128)S(1)} %pad_maximum_fusion.2), channel_id=1, source_target_pairs={{0,16},{8,24},{1,17},{9,25},{2,18},{10,26},{3,19},{11,27},{4,20},{... | collective-permute-start | bytes 49160 | tf_op jit(solution)/shard_map/ppermute | solution.py:530
  101.2 1.8 %collective-permute-start.19 = (f32[2,2,1024]{2,1,0:T(2,128)S(1)}, f32[2,2,1024]{2,1,0:T(2,128)S(1)}, u32[]{:S(2)}, u32[]{:S(2)}) collective-permute-start(f32[2,2,1024]{2,1,0:T(2,128)S(1)} %pad_maximum_fusion.2), channel_id=1, source_target_pairs={{0,24},{1,25},{2,26},{3,27},{4,28},{5,29},{6,30},{7,31}} | collective-permute-start | bytes 49160 | tf_op jit(solution)/shard_map/ppermute | solution.py:530
  103.0 5.6 %shard_map.138 = bf16[800,1024]{1,0:T(8,128)(2,1)S(1)} custom-call(bf16[800,2048]{1,0:T(8,128)(2,1)S(1)} %bitcast.76, bf16[1,128,1024]{2,1,0:T(8,128)(2,1)S(1)} %bitcast.71, bf16[1,128,1024]{2,1,0:T(8,128)(2,1)} %collective-permute-done.20.refs_1_, bf16[1,128,1024]{2,1,0:T(8,128)(2,1)} %collective-permute-done.21.refs_2_, ...), custom_call_target="tpu_custom_call" | custom-call | flops 3355443200 | bytes 4194304 | tf_op jit(solution)/shard_map/pallas_call | solution.py:165
  110.1 1.5 collective-permute-start.50
  112.3 3.3 %pool_mixed.1.refs_2_.refs_3_ = bf16[2,384,1024]{2,1,0:T(8,128)(2,1)S(1)} custom-call(s32[1]{0:T(128)} %bitcast.14.start, bf16[2,400,1024]{2,1,0:T(8,128)(2,1)S(1)} %bitcast.78, bf16[4,256,256]{2,1,0:T(8,128)(2,1)S(1)} %copy-done.4, f32[1,1024]{1,0:T(1,128)S(1)} %bitcast.74), custom_call_target="tpu_custom_call" | custom-call | flops 4000000000 | bytes 4000000 | tf_op jit(solution)/shard_map/pool_mixed/pallas_call | solution.py:306
  117.7 4.7 %collective-permute-done.50.refs_12_.refs_14_ = bf16[2,1024,128]{2,1,0:T(8,128)(2,1)S(1)} collective-permute-done((bf16[2,1024,128]{2,1,0:T(8,128)(2,1)S(1)}, bf16[2,1024,128]{2,1,0:T(8,128)(2,1)S(1)}, u32[]{:S(2)}, u32[]{:S(2)}) %collective-permute-start.50) | collective-permute-done | bytes 524320 | tf_op jit(solution)/shard_map/ppermute | solution.py:40
  123.0 7.8 %collective-permute-done.51.refs_14_.refs_16_ = bf16[2,1024,128]{2,1,0:T(8,128)(2,1)S(1)} collective-permute-done((bf16[2,1024,128]{2,1,0:T(8,128)(2,1)S(1)}, bf16[2,1024,128]{2,1,0:T(8,128)(2,1)S(1)}, u32[]{:S(2)}, u32[]{:S(2)}) %collective-permute-start.51) | collective-permute-done | bytes 524320 | tf_op jit(solution)/shard_map/ppermute | solution.py:40
  130.8 2.6 %shard_map.140 = bf16[2,192,1536]{2,1,0:T(8,128)(2,1)S(1)} custom-call(s32[1]{0:T(128)S(6)} %sub.16.refs_0_, bf16[2,384,1024]{2,1,0:T(8,128)(2,1)S(1)} %shard_map.137.refs_1_.refs_2_, bf16[2,384,1024]{2,1,0:T(8,128)(2,1)S(1)} %pool_mixed.1.refs_2_.refs_3_, bf16[2,1024,128]{2,1,0:T(8,128)(2,1)S(1)} %pad_maximum_fusion.refs_3_.refs_5_, ...), custom_call_target="tpu_custom_call" | custom-call | flops 2415919104 | bytes 6000000 | tf_op jit(solution)/shard_map/pallas_call | solution.py:451
  133.5 14.8 %collective-permute-start.52 = (bf16[2,192,1536]{2,1,0:T(8,128)(2,1)S(1)}, bf16[2,192,1536]{2,1,0:T(8,128)(2,1)S(1)}, u32[]{:S(2)}, u32[]{:S(2)}) collective-permute-start(bf16[2,192,1536]{2,1,0:T(8,128)(2,1)S(1)} %shard_map.140), channel_id=1, source_target_pairs={{0,1},{1,0},{2,3},{3,2},{4,5},{5,4},{6,7},{7,6},{8,9},{9,8},{10,11... | collective-permute-start | bytes 3538952 | tf_op jit(solution)/shard_map/ppermute | solution.py:543
  149.0 12.7 %collective-permute-done.39.refs_4_.refs_6_ = bf16[2,1024,128]{2,1,0:T(8,128)(2,1)S(1)} collective-permute-done((bf16[2,1024,128]{2,1,0:T(8,128)(2,1)S(1)}, bf16[2,1024,128]{2,1,0:T(8,128)(2,1)S(1)}, u32[]{:S(2)}, u32[]{:S(2)}) %collective-permute-start.39) | collective-permute-done | bytes 524320 | tf_op jit(solution)/shard_map/ppermute | solution.py:40
  161.7 1.0 shard_map.139
  162.7 1.2 collective-permute-start.45
  163.8 4.1 %shard_map.141.refs_9_ = bf16[2,192,2048]{2,1,0:T(8,128)(2,1)} custom-call(s32[16]{0:T(128)S(1)} %add.41.order.refs_0_, s32[1]{0:T(128)} %bitcast.side.refs_1_, bf16[2,384,1024]{2,1,0:T(8,128)(2,1)S(1)} %shard_map.137.refs_1_.refs_2_, bf16[2,384,1024]{2,1,0:T(8,128)(2,1)S(1)} %pool_mixed.1.refs_2_.refs_3_, ...), custom_call_target="tpu_custom_call" | custom-call | flops 2415919104 | bytes 6000000 | tf_op jit(solution)/shard_map/pallas_call | solution.py:451
  167.9 2.3 %shard_map.142 = bf16[2,192,2048]{2,1,0:T(8,128)(2,1)} custom-call(s32[16]{0:T(128)S(1)} %add.41.order.refs_0_, s32[1]{0:T(128)} %bitcast.side.refs_1_, bf16[2,384,1024]{2,1,0:T(8,128)(2,1)S(1)} %shard_map.137.refs_1_.refs_2_, bf16[2,384,1024]{2,1,0:T(8,128)(2,1)S(1)} %pool_mixed.1.refs_2_.refs_3_, ...), custom_call_target="tpu_custom_call", output_to_operand_aliasing={{}: (9, {})} | custom-call | flops 805306368 | bytes 6000000 | tf_op jit(solution)/shard_map/pallas_call | solution.py:451
  (108 shorter events, 19.5 us)
Async XLA Ops:
  0.0 34.7 %collective-permute-start = (bf16[2,192,2048]{2,1,0:T(8,128)(2,1)}, bf16[2,192,2048]{2,1,0:T(8,128)(2,1)S(1)}, u32[]{:S(2)}, u32[]{:S(2)}) collective-permute-start(bf16[2,192,2048]{2,1,0:T(8,128)(2,1)} %own.1), channel_id=1, source_target_pairs={{0,1},{1,0},{2,3},{3,2},{4,5},{5,4},{6,7},{7,6},{8,9},{9,8},{10,11... | collective-permute-start | bytes 4718600 | tf_op jit(solution)/shard_map/ppermute | solution.py:516
  0.0 11.7 %collective-permute-start.5 = (bf16[1,128,1024]{2,1,0:T(8,128)(2,1)}, bf16[1,128,1024]{2,1,0:T(8,128)(2,1)}, u32[]{:S(2)}, u32[]{:S(2)}) collective-permute-start(bf16[1,128,1024]{2,1,0:T(8,128)(2,1)} %bitcast.64), channel_id=1, source_target_pairs={{0,8},{8,16},{16,24},{24,0},{1,9},{9,17},{17,25},{25,1},{2,10},{10... | collective-permute-start | bytes 786440 | tf_op jit(solution)/shard_map/ppermute | solution.py:48
  2.8 10.0 %collective-permute-start.2 = (bf16[1,128,1024]{2,1,0:T(8,128)(2,1)}, bf16[1,128,1024]{2,1,0:T(8,128)(2,1)}, u32[]{:S(2)}, u32[]{:S(2)}) collective-permute-start(bf16[1,128,1024]{2,1,0:T(8,128)(2,1)} %bitcast.65), channel_id=1, source_target_pairs={{0,2},{2,0},{4,6},{6,4},{1,3},{3,1},{5,7},{7,5},{8,10},{10,8},{12,... | collective-permute-start | bytes 786440 | tf_op jit(solution)/shard_map/ppermute | solution.py:40
  4.0 10.0 %collective-permute-start.3 = (bf16[1,128,1024]{2,1,0:T(8,128)(2,1)}, bf16[1,128,1024]{2,1,0:T(8,128)(2,1)S(1)}, u32[]{:S(2)}, u32[]{:S(2)}) collective-permute-start(bf16[1,128,1024]{2,1,0:T(8,128)(2,1)} %bitcast.66), channel_id=1, source_target_pairs={{0,4},{2,6},{4,0},{6,2},{1,5},{3,7},{5,1},{7,3},{8,12},{10,14},{12... | collective-permute-start | bytes 786440 | tf_op jit(solution)/shard_map/ppermute | solution.py:40
  5.2 12.0 %collective-permute-start.23 = (bf16[1,128,1024]{2,1,0:T(8,128)(2,1)}, bf16[1,128,1024]{2,1,0:T(8,128)(2,1)S(1)}, u32[]{:S(2)}, u32[]{:S(2)}) collective-permute-start(bf16[1,128,1024]{2,1,0:T(8,128)(2,1)} %bitcast.68), channel_id=1, source_target_pairs={{0,8},{8,16},{16,24},{24,0},{1,9},{9,17},{17,25},{25,1},{2,10},{10... | collective-permute-start | bytes 786440 | tf_op jit(solution)/shard_map/ppermute | solution.py:48
  11.8 7.3 %collective-permute-start.20 = (bf16[1,128,1024]{2,1,0:T(8,128)(2,1)}, bf16[1,128,1024]{2,1,0:T(8,128)(2,1)}, u32[]{:S(2)}, u32[]{:S(2)}) collective-permute-start(bf16[1,128,1024]{2,1,0:T(8,128)(2,1)} %bitcast.69), channel_id=1, source_target_pairs={{0,2},{2,0},{4,6},{6,4},{1,3},{3,1},{5,7},{7,5},{8,10},{10,8},{12,... | collective-permute-start | bytes 786440 | tf_op jit(solution)/shard_map/ppermute | solution.py:40
  14.7 10.3 %collective-permute-start.35 = (bf16[1,1024,128]{2,1,0:T(8,128)(2,1)}, bf16[1,1024,128]{2,1,0:T(8,128)(2,1)}, u32[]{:S(2)}, u32[]{:S(2)}) collective-permute-start(bf16[1,1024,128]{2,1,0:T(8,128)(2,1)} %bitcast.79), channel_id=1, source_target_pairs={{0,4},{2,6},{4,0},{6,2},{1,5},{3,7},{5,1},{7,3},{8,12},{10,14},{12... | collective-permute-start | bytes 786440 | tf_op jit(solution)/shard_map/ppermute | solution.py:40
  17.3 9.3 %collective-permute-start.9 = (bf16[1,128,1024]{2,1,0:T(8,128)(2,1)}, bf16[1,128,1024]{2,1,0:T(8,128)(2,1)}, u32[]{:S(2)}, u32[]{:S(2)}) collective-permute-start(bf16[1,128,1024]{2,1,0:T(8,128)(2,1)} %collective-permute-done.5.refs_4_), channel_id=1, source_target_pairs={{0,8},{8,16},{16,24},{24,0},{1,9},{9,17},{17,25},{25,1},{2,10},{10... | collective-permute-start | bytes 786440 | tf_op jit(solution)/shard_map/ppermute | solution.py:48
  19.1 7.7 %collective-permute-start.40 = (bf16[1,1024,128]{2,1,0:T(8,128)(2,1)}, bf16[1,1024,128]{2,1,0:T(8,128)(2,1)}, u32[]{:S(2)}, u32[]{:S(2)}) collective-permute-start(bf16[1,1024,128]{2,1,0:T(8,128)(2,1)} %bitcast.81), channel_id=1, source_target_pairs={{0,2},{2,0},{4,6},{6,4},{1,3},{3,1},{5,7},{7,5},{8,10},{10,8},{12,... | collective-permute-start | bytes 786440 | tf_op jit(solution)/shard_map/ppermute | solution.py:40
  19.6 11.0 %collective-permute-start.6 = (bf16[1,128,1024]{2,1,0:T(8,128)(2,1)}, bf16[1,128,1024]{2,1,0:T(8,128)(2,1)}, u32[]{:S(2)}, u32[]{:S(2)}) collective-permute-start(bf16[1,128,1024]{2,1,0:T(8,128)(2,1)} %collective-permute-done.5.refs_4_), channel_id=1, source_target_pairs={{0,4},{2,6},{4,0},{6,2},{1,5},{3,7},{5,1},{7,3},{8,12},{10,14},{12... | collective-permute-start | bytes 786440 | tf_op jit(solution)/shard_map/ppermute | solution.py:40
  26.6 7.3 %collective-permute-start.13 = (bf16[1,128,1024]{2,1,0:T(8,128)(2,1)}, bf16[1,128,1024]{2,1,0:T(8,128)(2,1)}, u32[]{:S(2)}, u32[]{:S(2)}) collective-permute-start(bf16[1,128,1024]{2,1,0:T(8,128)(2,1)} %collective-permute-done.9.refs_8_), channel_id=1, source_target_pairs={{0,8},{8,16},{16,24},{24,0},{1,9},{9,17},{17,25},{25,1},{2,10},{10... | collective-permute-start | bytes 786440 | tf_op jit(solution)/shard_map/ppermute | solution.py:48
  26.8 18.3 %collective-permute-start.27 = (bf16[1,128,1024]{2,1,0:T(8,128)(2,1)S(1)}, bf16[1,128,1024]{2,1,0:T(8,128)(2,1)S(1)}, u32[]{:S(2)}, u32[]{:S(2)}) collective-permute-start(bf16[1,128,1024]{2,1,0:T(8,128)(2,1)S(1)} %collective-permute-done.23.refs_4_), channel_id=1, source_target_pairs={{0,8},{8,16},{16,24},{24,0},{1,9},{9,17},{17,25},{25,1},{2,10},{10... | collective-permute-start | bytes 786440 | tf_op jit(solution)/shard_map/ppermute | solution.py:48
  30.6 15.8 %collective-permute-start.24 = (bf16[1,128,1024]{2,1,0:T(8,128)(2,1)S(1)}, bf16[1,128,1024]{2,1,0:T(8,128)(2,1)S(1)}, u32[]{:S(2)}, u32[]{:S(2)}) collective-permute-start(bf16[1,128,1024]{2,1,0:T(8,128)(2,1)S(1)} %collective-permute-done.23.refs_4_), channel_id=1, source_target_pairs={{0,4},{2,6},{4,0},{6,2},{1,5},{3,7},{5,1},{7,3},{8,12},{10,14},{12... | collective-permute-start | bytes 786440 | tf_op jit(solution)/shard_map/ppermute | solution.py:40
  31.8 9.8 %collective-permute-start.4 = (bf16[1,128,1024]{2,1,0:T(8,128)(2,1)}, bf16[1,128,1024]{2,1,0:T(8,128)(2,1)S(1)}, u32[]{:S(2)}, u32[]{:S(2)}) collective-permute-start(bf16[1,128,1024]{2,1,0:T(8,128)(2,1)} %collective-permute-done.2.refs_1_), channel_id=1, source_target_pairs={{0,4},{2,6},{4,0},{6,2},{1,5},{3,7},{5,1},{7,3},{8,12},{10,14},{12... | collective-permute-start | bytes 786440 | tf_op jit(solution)/shard_map/ppermute | solution.py:40
  33.9 13.6 %collective-permute-start.10 = (bf16[1,128,1024]{2,1,0:T(8,128)(2,1)}, bf16[1,128,1024]{2,1,0:T(8,128)(2,1)S(1)}, u32[]{:S(2)}, u32[]{:S(2)}) collective-permute-start(bf16[1,128,1024]{2,1,0:T(8,128)(2,1)} %collective-permute-done.9.refs_8_), channel_id=1, source_target_pairs={{0,2},{2,0},{4,6},{6,4},{1,3},{3,1},{5,7},{7,5},{8,10},{10,8},{12,... | collective-permute-start | bytes 786440 | tf_op jit(solution)/shard_map/ppermute | solution.py:40
  34.7 13.1 %collective-permute-start.14 = (bf16[1,128,1024]{2,1,0:T(8,128)(2,1)}, bf16[1,128,1024]{2,1,0:T(8,128)(2,1)S(1)}, u32[]{:S(2)}, u32[]{:S(2)}) collective-permute-start(bf16[1,128,1024]{2,1,0:T(8,128)(2,1)} %collective-permute-done.13.refs_12_), channel_id=1, source_target_pairs={{0,4},{2,6},{4,0},{6,2},{1,5},{3,7},{5,1},{7,3},{8,12},{10,14},{12... | collective-permute-start | bytes 786440 | tf_op jit(solution)/shard_map/ppermute | solution.py:40
  45.1 7.6 %collective-permute-start.11 = (bf16[1,128,1024]{2,1,0:T(8,128)(2,1)}, bf16[1,128,1024]{2,1,0:T(8,128)(2,1)S(1)}, u32[]{:S(2)}, u32[]{:S(2)}) collective-permute-start(bf16[1,128,1024]{2,1,0:T(8,128)(2,1)} %collective-permute-done.9.refs_8_), channel_id=1, source_target_pairs={{0,4},{2,6},{4,0},{6,2},{1,5},{3,7},{5,1},{7,3},{8,12},{10,14},{12... | collective-permute-start | bytes 786440 | tf_op jit(solution)/shard_map/ppermute | solution.py:40
  47.6 7.4 %collective-permute-start.15 = (bf16[1,128,1024]{2,1,0:T(8,128)(2,1)}, bf16[1,128,1024]{2,1,0:T(8,128)(2,1)S(1)}, u32[]{:S(2)}, u32[]{:S(2)}) collective-permute-start(bf16[1,128,1024]{2,1,0:T(8,128)(2,1)} %collective-permute-done.13.refs_12_), channel_id=1, source_target_pairs={{0,2},{2,0},{4,6},{6,4},{1,3},{3,1},{5,7},{7,5},{8,10},{10,8},{12,... | collective-permute-start | bytes 786440 | tf_op jit(solution)/shard_map/ppermute | solution.py:40
  47.9 8.8 %collective-permute-start.12 = (bf16[1,128,1024]{2,1,0:T(8,128)(2,1)S(1)}, bf16[1,128,1024]{2,1,0:T(8,128)(2,1)S(1)}, u32[]{:S(2)}, u32[]{:S(2)}) collective-permute-start(bf16[1,128,1024]{2,1,0:T(8,128)(2,1)S(1)} %collective-permute-done.10.refs_9_), channel_id=1, source_target_pairs={{0,4},{2,6},{4,0},{6,2},{1,5},{3,7},{5,1},{7,3},{8,12},{10,14},{12... | collective-permute-start | bytes 786440 | tf_op jit(solution)/shard_map/ppermute | solution.py:40
  48.5 10.7 %collective-permute-start.16 = (bf16[1,128,1024]{2,1,0:T(8,128)(2,1)S(1)}, bf16[1,128,1024]{2,1,0:T(8,128)(2,1)S(1)}, u32[]{:S(2)}, u32[]{:S(2)}) collective-permute-start(bf16[1,128,1024]{2,1,0:T(8,128)(2,1)S(1)} %collective-permute-done.14.refs_13_), channel_id=1, source_target_pairs={{0,2},{2,0},{4,6},{6,4},{1,3},{3,1},{5,7},{7,5},{8,10},{10,8},{12,... | collective-permute-start | bytes 786440 | tf_op jit(solution)/shard_map/ppermute | solution.py:40
  52.7 12.7 %collective-permute-start.25 = (bf16[1,128,1024]{2,1,0:T(8,128)(2,1)S(1)}, bf16[1,128,1024]{2,1,0:T(8,128)(2,1)S(1)}, u32[]{:S(2)}, u32[]{:S(2)}) collective-permute-start(bf16[1,128,1024]{2,1,0:T(8,128)(2,1)S(1)} %collective-permute-done.23.refs_4_), channel_id=1, source_target_pairs={{0,2},{2,0},{4,6},{6,4},{1,3},{3,1},{5,7},{7,5},{8,10},{10,8},{12,... | collective-permute-start | bytes 786440 | tf_op jit(solution)/shard_map/ppermute | solution.py:40
  53.6 11.9 %collective-permute-start.22 = (bf16[1,128,1024]{2,1,0:T(8,128)(2,1)}, bf16[1,128,1024]{2,1,0:T(8,128)(2,1)S(1)}, u32[]{:S(2)}, u32[]{:S(2)}) collective-permute-start(bf16[1,128,1024]{2,1,0:T(8,128)(2,1)} %collective-permute-done.20.refs_1_), channel_id=1, source_target_pairs={{0,4},{2,6},{4,0},{6,2},{1,5},{3,7},{5,1},{7,3},{8,12},{10,14},{12... | collective-permute-start | bytes 786440 | tf_op jit(solution)/shard_map/ppermute | solution.py:40
  54.9 11.7 %collective-permute-start.31 = (bf16[1,128,1024]{2,1,0:T(8,128)(2,1)S(1)}, bf16[1,128,1024]{2,1,0:T(8,128)(2,1)S(1)}, u32[]{:S(2)}, u32[]{:S(2)}) collective-permute-start(bf16[1,128,1024]{2,1,0:T(8,128)(2,1)S(1)} %collective-permute-done.27.refs_8_), channel_id=1, source_target_pairs={{0,8},{8,16},{16,24},{24,0},{1,9},{9,17},{17,25},{25,1},{2,10},{10... | collective-permute-start | bytes 786440 | tf_op jit(solution)/shard_map/ppermute | solution.py:48
  56.7 13.7 %collective-permute-start.28 = (bf16[1,128,1024]{2,1,0:T(8,128)(2,1)S(1)}, bf16[1,128,1024]{2,1,0:T(8,128)(2,1)S(1)}, u32[]{:S(2)}, u32[]{:S(2)}) collective-permute-start(bf16[1,128,1024]{2,1,0:T(8,128)(2,1)S(1)} %collective-permute-done.27.refs_8_), channel_id=1, source_target_pairs={{0,2},{2,0},{4,6},{6,4},{1,3},{3,1},{5,7},{7,5},{8,10},{10,8},{12,... | collective-permute-start | bytes 786440 | tf_op jit(solution)/shard_map/ppermute | solution.py:40
  59.2 12.1 %collective-permute-start.29 = (bf16[1,128,1024]{2,1,0:T(8,128)(2,1)S(1)}, bf16[1,128,1024]{2,1,0:T(8,128)(2,1)S(1)}, u32[]{:S(2)}, u32[]{:S(2)}) collective-permute-start(bf16[1,128,1024]{2,1,0:T(8,128)(2,1)S(1)} %collective-permute-done.27.refs_8_), channel_id=1, source_target_pairs={{0,4},{2,6},{4,0},{6,2},{1,5},{3,7},{5,1},{7,3},{8,12},{10,14},{12... | collective-permute-start | bytes 786440 | tf_op jit(solution)/shard_map/ppermute | solution.py:40
  65.4 22.3 %collective-permute-start.36 = (bf16[2,1024,128]{2,1,0:T(8,128)(2,1)S(1)}, bf16[2,1024,128]{2,1,0:T(8,128)(2,1)S(1)}, u32[]{:S(2)}, u32[]{:S(2)}) collective-permute-start(bf16[2,1024,128]{2,1,0:T(8,128)(2,1)S(1)} %pad_maximum_fusion.refs_3_.refs_5_), channel_id=1, source_target_pairs={{0,8},{8,16},{16,24},{24,0},{1,9},{9,17},{17,25},{25,1},{2,10},{10... | collective-permute-start | bytes 1572872 | tf_op jit(solution)/shard_map/ppermute | solution.py:70
  65.4 23.1 %collective-permute-start.46 = (bf16[2,1024,128]{2,1,0:T(8,128)(2,1)S(1)}, bf16[2,1024,128]{2,1,0:T(8,128)(2,1)S(1)}, u32[]{:S(2)}, u32[]{:S(2)}) collective-permute-start(bf16[2,1024,128]{2,1,0:T(8,128)(2,1)S(1)} %pad_maximum_fusion.refs_3_.refs_5_), channel_id=1, source_target_pairs={{0,2},{2,0},{4,6},{6,4},{1,3},{3,1},{5,7},{7,5},{8,10},{10,8},{12,... | collective-permute-start | bytes 1572872 | tf_op jit(solution)/shard_map/ppermute | solution.py:40
  66.6 21.0 %collective-permute-start.41 = (bf16[2,1024,128]{2,1,0:T(8,128)(2,1)S(1)}, bf16[2,1024,128]{2,1,0:T(8,128)(2,1)S(1)}, u32[]{:S(2)}, u32[]{:S(2)}) collective-permute-start(bf16[2,1024,128]{2,1,0:T(8,128)(2,1)S(1)} %pad_maximum_fusion.1.refs_9_.refs_11_), channel_id=1, source_target_pairs={{0,8},{8,16},{16,24},{24,0},{1,9},{9,17},{17,25},{25,1},{2,10},{10... | collective-permute-start | bytes 1572872 | tf_op jit(solution)/shard_map/ppermute | solution.py:70
  70.4 16.6 %collective-permute-start.26 = (bf16[1,128,1024]{2,1,0:T(8,128)(2,1)S(1)}, bf16[1,128,1024]{2,1,0:T(8,128)(2,1)S(1)}, u32[]{:S(2)}, u32[]{:S(2)}) collective-permute-start(bf16[1,128,1024]{2,1,0:T(8,128)(2,1)S(1)} %collective-permute-done.24.refs_5_), channel_id=1, source_target_pairs={{0,2},{2,0},{4,6},{6,4},{1,3},{3,1},{5,7},{7,5},{8,10},{10,8},{12,... | collective-permute-start | bytes 786440 | tf_op jit(solution)/shard_map/ppermute | solution.py:40
  71.2 18.4 %collective-permute-start.32 = (bf16[1,128,1024]{2,1,0:T(8,128)(2,1)S(1)}, bf16[1,128,1024]{2,1,0:T(8,128)(2,1)S(1)}, u32[]{:S(2)}, u32[]{:S(2)}) collective-permute-start(bf16[1,128,1024]{2,1,0:T(8,128)(2,1)S(1)} %collective-permute-done.31.refs_12_), channel_id=1, source_target_pairs={{0,4},{2,6},{4,0},{6,2},{1,5},{3,7},{5,1},{7,3},{8,12},{10,14},{12... | collective-permute-start | bytes 786440 | tf_op jit(solution)/shard_map/ppermute | solution.py:40
  87.0 8.3 %collective-permute-start.33 = (bf16[1,128,1024]{2,1,0:T(8,128)(2,1)S(1)}, bf16[1,128,1024]{2,1,0:T(8,128)(2,1)S(1)}, u32[]{:S(2)}, u32[]{:S(2)}) collective-permute-start(bf16[1,128,1024]{2,1,0:T(8,128)(2,1)S(1)} %collective-permute-done.31.refs_12_), channel_id=1, source_target_pairs={{0,2},{2,0},{4,6},{6,4},{1,3},{3,1},{5,7},{7,5},{8,10},{10,8},{12,... | collective-permute-start | bytes 786440 | tf_op jit(solution)/shard_map/ppermute | solution.py:40
  87.7 9.6 %collective-permute-start.30 = (bf16[1,128,1024]{2,1,0:T(8,128)(2,1)S(1)}, bf16[1,128,1024]{2,1,0:T(8,128)(2,1)S(1)}, u32[]{:S(2)}, u32[]{:S(2)}) collective-permute-start(bf16[1,128,1024]{2,1,0:T(8,128)(2,1)S(1)} %collective-permute-done.28.refs_9_), channel_id=1, source_target_pairs={{0,4},{2,6},{4,0},{6,2},{1,5},{3,7},{5,1},{7,3},{8,12},{10,14},{12... | collective-permute-start | bytes 786440 | tf_op jit(solution)/shard_map/ppermute | solution.py:40
  87.7 21.0 %collective-permute-start.37 = (bf16[2,1024,128]{2,1,0:T(8,128)(2,1)S(1)}, bf16[2,1024,128]{2,1,0:T(8,128)(2,1)S(1)}, u32[]{:S(2)}, u32[]{:S(2)}) collective-permute-start(bf16[2,1024,128]{2,1,0:T(8,128)(2,1)S(1)} %collective-permute-done.36.refs_5_.refs_7_), channel_id=1, source_target_pairs={{0,8},{8,16},{16,24},{24,0},{1,9},{9,17},{17,25},{25,1},{2,10},{10... | collective-permute-start | bytes 1572872 | tf_op jit(solution)/shard_map/ppermute | solution.py:70
  88.5 20.8 %collective-permute-start.42 = (bf16[2,1024,128]{2,1,0:T(8,128)(2,1)S(1)}, bf16[2,1024,128]{2,1,0:T(8,128)(2,1)S(1)}, u32[]{:S(2)}, u32[]{:S(2)}) collective-permute-start(bf16[2,1024,128]{2,1,0:T(8,128)(2,1)S(1)} %collective-permute-done.41.refs_11_.refs_13_), channel_id=1, source_target_pairs={{0,8},{8,16},{16,24},{24,0},{1,9},{9,17},{17,25},{25,1},{2,10},{10... | collective-permute-start | bytes 1572872 | tf_op jit(solution)/shard_map/ppermute | solution.py:70
  89.6 11.6 %collective-permute-start.34 = (bf16[1,128,1024]{2,1,0:T(8,128)(2,1)S(1)}, bf16[1,128,1024]{2,1,0:T(8,128)(2,1)S(1)}, u32[]{:S(2)}, u32[]{:S(2)}) collective-permute-start(bf16[1,128,1024]{2,1,0:T(8,128)(2,1)S(1)} %collective-permute-done.32.refs_13_), channel_id=1, source_target_pairs={{0,2},{2,0},{4,6},{6,4},{1,3},{3,1},{5,7},{7,5},{8,10},{10,8},{12,... | collective-permute-start | bytes 786440 | tf_op jit(solution)/shard_map/ppermute | solution.py:40
  95.4 14.7 %collective-permute-start.17 = (f32[2,2,1024]{2,1,0:T(2,128)S(1)}, f32[2,2,1024]{2,1,0:T(2,128)S(1)}, u32[]{:S(2)}, u32[]{:S(2)}) collective-permute-start(f32[2,2,1024]{2,1,0:T(2,128)S(1)} %pad_maximum_fusion.2), channel_id=1, source_target_pairs={{0,8},{8,16},{16,24},{1,9},{9,17},{17,25},{2,10},{10,18},{18,26},{... | collective-permute-start | bytes 49160 | tf_op jit(solution)/shard_map/ppermute | solution.py:530
  97.3 14.4 %collective-permute-start.18 = (f32[2,2,1024]{2,1,0:T(2,128)S(1)}, f32[2,2,1024]{2,1,0:T(2,128)S(1)}, u32[]{:S(2)}, u32[]{:S(2)}) collective-permute-start(f32[2,2,1024]{2,1,0:T(2,128)S(1)} %pad_maximum_fusion.2), channel_id=1, source_target_pairs={{0,16},{8,24},{1,17},{9,25},{2,18},{10,26},{3,19},{11,27},{4,20},{... | collective-permute-start | bytes 49160 | tf_op jit(solution)/shard_map/ppermute | solution.py:530
  101.2 10.5 %collective-permute-start.19 = (f32[2,2,1024]{2,1,0:T(2,128)S(1)}, f32[2,2,1024]{2,1,0:T(2,128)S(1)}, u32[]{:S(2)}, u32[]{:S(2)}) collective-permute-start(f32[2,2,1024]{2,1,0:T(2,128)S(1)} %pad_maximum_fusion.2), channel_id=1, source_target_pairs={{0,24},{1,25},{2,26},{3,27},{4,28},{5,29},{6,30},{7,31}} | collective-permute-start | bytes 49160 | tf_op jit(solution)/shard_map/ppermute | solution.py:530
  108.7 8.4 %collective-permute-start.49 = (bf16[2,1024,128]{2,1,0:T(8,128)(2,1)S(1)}, bf16[2,1024,128]{2,1,0:T(8,128)(2,1)S(1)}, u32[]{:S(2)}, u32[]{:S(2)}) collective-permute-start(bf16[2,1024,128]{2,1,0:T(8,128)(2,1)S(1)} %pad_maximum_fusion.1.refs_9_.refs_11_), channel_id=1, source_target_pairs={{0,4},{2,6},{4,0},{6,2},{1,5},{3,7},{5,1},{7,3},{8,12},{10,14},{12... | collective-permute-start | bytes 1572872 | tf_op jit(solution)/shard_map/ppermute | solution.py:40
  109.4 8.3 %collective-permute-start.47 = (bf16[2,1024,128]{2,1,0:T(8,128)(2,1)S(1)}, bf16[2,1024,128]{2,1,0:T(8,128)(2,1)S(1)}, u32[]{:S(2)}, u32[]{:S(2)}) collective-permute-start(bf16[2,1024,128]{2,1,0:T(8,128)(2,1)S(1)} %collective-permute-done.36.refs_5_.refs_7_), channel_id=1, source_target_pairs={{0,2},{2,0},{4,6},{6,4},{1,3},{3,1},{5,7},{7,5},{8,10},{10,8},{12,... | collective-permute-start | bytes 1572872 | tf_op jit(solution)/shard_map/ppermute | solution.py:40
  110.1 12.4 %collective-permute-start.50 = (bf16[2,1024,128]{2,1,0:T(8,128)(2,1)S(1)}, bf16[2,1024,128]{2,1,0:T(8,128)(2,1)S(1)}, u32[]{:S(2)}, u32[]{:S(2)}) collective-permute-start(bf16[2,1024,128]{2,1,0:T(8,128)(2,1)S(1)} %collective-permute-done.41.refs_11_.refs_13_), channel_id=1, source_target_pairs={{0,4},{2,6},{4,0},{6,2},{1,5},{3,7},{5,1},{7,3},{8,12},{10,14},{12... | collective-permute-start | bytes 1572872 | tf_op jit(solution)/shard_map/ppermute | solution.py:40
  111.6 11.4 %collective-permute-start.48 = (bf16[2,1024,128]{2,1,0:T(8,128)(2,1)S(1)}, bf16[2,1024,128]{2,1,0:T(8,128)(2,1)S(1)}, u32[]{:S(2)}, u32[]{:S(2)}) collective-permute-start(bf16[2,1024,128]{2,1,0:T(8,128)(2,1)S(1)} %collective-permute-done.37.refs_7_.refs_9_), channel_id=1, source_target_pairs={{0,2},{2,0},{4,6},{6,4},{1,3},{3,1},{5,7},{7,5},{8,10},{10,8},{12,... | collective-permute-start | bytes 1572872 | tf_op jit(solution)/shard_map/ppermute | solution.py:40
  111.7 19.1 %collective-permute-start.51 = (bf16[2,1024,128]{2,1,0:T(8,128)(2,1)S(1)}, bf16[2,1024,128]{2,1,0:T(8,128)(2,1)S(1)}, u32[]{:S(2)}, u32[]{:S(2)}) collective-permute-start(bf16[2,1024,128]{2,1,0:T(8,128)(2,1)S(1)} %collective-permute-done.42.refs_13_.refs_15_), channel_id=1, source_target_pairs={{0,4},{2,6},{4,0},{6,2},{1,5},{3,7},{5,1},{7,3},{8,12},{10,14},{12... | collective-permute-start | bytes 1572872 | tf_op jit(solution)/shard_map/ppermute | solution.py:40
  117.1 31.2 %collective-permute-start.38 = (bf16[2,1024,128]{2,1,0:T(8,128)(2,1)S(1)}, bf16[2,1024,128]{2,1,0:T(8,128)(2,1)S(1)}, u32[]{:S(2)}, u32[]{:S(2)}) collective-permute-start(bf16[2,1024,128]{2,1,0:T(8,128)(2,1)S(1)} %collective-permute-done.37.refs_7_.refs_9_), channel_id=1, source_target_pairs={{0,8},{8,16},{16,24},{24,0},{1,9},{9,17},{17,25},{25,1},{2,10},{10... | collective-permute-start | bytes 1572872 | tf_op jit(solution)/shard_map/ppermute | solution.py:70
  117.7 30.7 %collective-permute-start.43 = (bf16[2,1024,128]{2,1,0:T(8,128)(2,1)S(1)}, bf16[2,1024,128]{2,1,0:T(8,128)(2,1)S(1)}, u32[]{:S(2)}, u32[]{:S(2)}) collective-permute-start(bf16[2,1024,128]{2,1,0:T(8,128)(2,1)S(1)} %collective-permute-done.42.refs_13_.refs_15_), channel_id=1, source_target_pairs={{0,8},{8,16},{16,24},{24,0},{1,9},{9,17},{17,25},{25,1},{2,10},{10... | collective-permute-start | bytes 1572872 | tf_op jit(solution)/shard_map/ppermute | solution.py:70
  133.5 30.4 %collective-permute-start.52 = (bf16[2,192,1536]{2,1,0:T(8,128)(2,1)S(1)}, bf16[2,192,1536]{2,1,0:T(8,128)(2,1)S(1)}, u32[]{:S(2)}, u32[]{:S(2)}) collective-permute-start(bf16[2,192,1536]{2,1,0:T(8,128)(2,1)S(1)} %shard_map.140), channel_id=1, source_target_pairs={{0,1},{1,0},{2,3},{3,2},{4,5},{5,4},{6,7},{7,6},{8,9},{9,8},{10,11... | collective-permute-start | bytes 3538952 | tf_op jit(solution)/shard_map/ppermute | solution.py:543
  148.3 13.4 %collective-permute-start.39 = (bf16[2,1024,128]{2,1,0:T(8,128)(2,1)S(1)}, bf16[2,1024,128]{2,1,0:T(8,128)(2,1)S(1)}, u32[]{:S(2)}, u32[]{:S(2)}) collective-permute-start(bf16[2,1024,128]{2,1,0:T(8,128)(2,1)S(1)} %collective-permute-done.38.refs_3_.refs_5_), channel_id=1, source_target_pairs={{0,2},{2,0},{4,6},{6,4},{1,3},{3,1},{5,7},{7,5},{8,10},{10,8},{12,... | collective-permute-start | bytes 1572872 | tf_op jit(solution)/shard_map/ppermute | solution.py:40
  148.4 13.2 %collective-permute-start.44 = (bf16[2,1024,128]{2,1,0:T(8,128)(2,1)S(1)}, bf16[2,1024,128]{2,1,0:T(8,128)(2,1)S(1)}, u32[]{:S(2)}, u32[]{:S(2)}) collective-permute-start(bf16[2,1024,128]{2,1,0:T(8,128)(2,1)S(1)} %collective-permute-done.43.refs_5_.refs_7_), channel_id=1, source_target_pairs={{0,4},{2,6},{4,0},{6,2},{1,5},{3,7},{5,1},{7,3},{8,12},{10,14},{12... | collective-permute-start | bytes 1572872 | tf_op jit(solution)/shard_map/ppermute | solution.py:40
  (19 other events, 291.3 us)
where the time goes:
time: 171 us; the launch traced here: 170 us
  waiting for transfers between devices  66.1 us (39%)
  starting transfers between devices  58.9 us (34%)
  Pallas kernels  40.6 us (24%)
  other arithmetic  3.2 us (2%)
    ppermute x34, waiting for transfers between devices, swapped(): came = lax.ppermute(stack, 'fs', swap_pairs(fs_n, bit))  55.9 us
    ppermute x34, starting transfers between devices, swapped(): came = lax.ppermute(stack, 'fs', swap_pairs(fs_n, bit))  26.3 us
    ppermute x1, starting transfers between devices, per_device(): came_early = lax.ppermute(ex(other_side, early), 'tp', swap_tp)  14.8 us
    pallas_call x1, Pallas kernels, chain_scan(): pl.pallas_call(functools.partial(chain_kernel, length), out_shape=(jax.Sh...  12.3 us
    pallas_call x2, Pallas kernels, entry_dot(): pl.pallas_call(functools.partial(entry_kernel, [places for _, places in p...  11.5 us
    ppermute x6, waiting for transfers between devices, gather_part(): held = (lax.ppermute(held[0], 'sp', ring), [(0, lap)])  10.2 us
    pallas_call x4, Pallas kernels, exit_columns(): pl.pallas_call(functools.partial(exit_kernel, chain_spots, pool_spots, co...  9.98 us
    ppermute x3, starting transfers between devices, per_device(): came = lax.ppermute(last, 'sp', [(i, i + back) for i in range(sp_n - back)])  7.62 us
  transfers between devices with their start and end apart: 53, of which 21 were waited for; matrix products, arithmetic and copies ran while one was open for 2% of the time, Pallas kernels for 22%

commit v1 on v0

--- a/solution.py
+++ b/solution.py
@@ -14,7 +14,7 @@
 RECUR_SCALE = 8.0
 CHUNKS = 8
 MIB = 1024 * 1024
-ROUTES = {"E1": ("xy", "yx", "xy", "yx"), "E2": ("xy", "yx", "xy", "yx"), "X1": "yzx", "X2": "xzy"}
+ROUTES = {"E1": ("xyx", "xyy", "xyx", "xyy"), "E2": ("xyx", "xyy", "xyx", "xyy"), "X1": "yzx", "X2": "xzy"}
 LATE_LAPS = 1
 
 
@@ -42,18 +42,28 @@
 
     found = []
     if isinstance(route, tuple):
-        held = (own, [(0, 0)])
+        past = None
         for lap in range(sp_n):
+            from_x, from_y, from_both = route[lap % len(route)]
+
+            def along(step, near, kind):
+                if step == "z":
+                    stack = lax.ppermute(past[kind][0], "sp", ring)
+                    return stack, [(f, lap) for f, _ in past[kind][1]]
+                return swapped(near, step)
+
+            held = (own, [(0, 0)])
             if lap:
-                held = (lax.ppermute(held[0], "sp", ring), [(0, lap)])
-            one, two = route[lap % len(route)]
-            first = swapped(held, one)
-            found += [held, first]
-            found += [swapped(held, two), swapped(first, two)]
+                held = (lax.ppermute(past[0][0], "sp", ring), [(0, lap)])
+            over_x = along(from_x, held, 1)
+            over_y = along(from_y, held, 2)
+            both = along(from_both, over_y if from_both == "x" else over_x, 3)
+            past = [held, over_x, over_y, both]
+            found += past
     elif route[0] == "z":
         one, two = route[1], route[2]
         laps = [own]
-        for _ in range(1, sp_n):
+        for lap in range(1, sp_n):
             laps.append(lax.ppermute(laps[-1], "sp", ring))
         for group in (range(0, sp_n // 2), range(sp_n // 2, sp_n)):
             held = join([laps[i] for i in group])
@@ -73,12 +83,12 @@
     return [(stack, [f * sp_n + s for f, s in places]) for stack, places in found]
 
 
-def norm_kernel(order, side, own, other, halo, gain, out):
+def norm_kernel(order, spot, own, other, halo, gain, out):
     blocks = own.shape[2] // LANES
     half = own.shape[1]
     width = own.shape[2]
 
-    def rows_of(src, base, count, size):
+    def rows_of(src, base, count, size, keep=None):
         def one(i, _):
             at = pl.multiple_of(i * size, size)
             squares = None
@@ -86,7 +96,10 @@
                 part = src[0, pl.ds(at, size), b * LANES : (b + 1) * LANES].astype(jnp.float32)
                 squares = part * part if squares is None else squares + part * part
             mean = jnp.sum(squares, axis=-1, keepdims=True) * (1.0 / width)
-            scale = jnp.broadcast_to(lax.rsqrt(mean + NORM_EPSILON), (size, LANES))
+            scale = lax.rsqrt(mean + NORM_EPSILON)
+            if keep is not None:
+                scale = scale * keep
+            scale = jnp.broadcast_to(scale, (size, LANES))
             to = pl.multiple_of(base + i * size, HALO)
             for b in range(blocks):
                 col = pl.multiple_of(order[b] * LANES, LANES)
@@ -99,12 +112,12 @@
         lax.fori_loop(0, count, one, 0)
 
     size = 64 if half % 64 == 0 else HALO
-    rows_of(halo, 0, 1, HALO)
-    rows_of(own, HALO + side[0] * half, half // size, size)
-    rows_of(other, HALO + (1 - side[0]) * half, half // size, size)
-
-
-def norm_rows(order, side, own, other, halo, gain):
+    rows_of(halo, 0, 1, HALO, jnp.where(spot[1] > 0, 1.0, 0.0))
+    rows_of(own, HALO + spot[0] * half, half // size, size)
+    rows_of(other, HALO + (1 - spot[0]) * half, half // size, size)
+
+
+def norm_rows(order, spot, own, other, halo, gain):
     seqs, half, width = own.shape
     rows = 2 * half + HALO
     return pl.pallas_call(
@@ -121,10 +134,10 @@
             ],
             out_specs=pl.BlockSpec((1, rows, width), lambda i, *_: (i, 0, 0)),
         ),
-        compiler_params=pltpu.CompilerParams(vmem_limit_bytes=24 * MIB),
+        compiler_params=pltpu.CompilerParams(vmem_limit_bytes=12 * MIB),
         cost_estimate=pl.CostEstimate(flops=4_000_000_000, transcendentals=0, bytes_accessed=8_000_000),
         name="norm_rows",
-    )(order, side, own, other, halo, gain.reshape(1, width))
+    )(order, spot, own, other, halo, gain.reshape(1, width))
 
 
 def entry_kernel(places, seqs, x, *refs):
@@ -172,42 +185,51 @@
             pltpu.VMEM((width // tile, depth, tile), jnp.bfloat16),
             pltpu.SemaphoreType.DMA((width // tile, shards)),
         ],
-        compiler_params=pltpu.CompilerParams(vmem_limit_bytes=20 * MIB),
+        compiler_params=pltpu.CompilerParams(vmem_limit_bytes=14 * MIB),
         cost_estimate=pl.CostEstimate(
             flops=2 * rows * depth * width, transcendentals=0, bytes_accessed=2 * depth * width
         ),
     )(x.reshape(rows, depth), *[stack for stack, _ in parts]).reshape(seqs, total, width)
 
 
-def chain_kernel(length, x, taps, wr, wi, rate_log, shift, h_out, p_out, seam_h, seam_p, wide):
+def chain_kernel(
+    length, x, taps, wr, wi, rate_log, shift, h_out, p_out, seam_h, seam_p, wide, conv_at, to_recur, to_input
+):
     rows = shift.shape[1]
     span = rows // CHUNKS
+    width = wide.shape[1]
     tap_count = taps.shape[0]
+    first = HALO - (tap_count - 1)
+    lanes = [slice(b * LANES, (b + 1) * LANES) for b in range(width // LANES)]
     wide[...] = x[0].astype(jnp.float32)
-    first = HALO - (tap_count - 1)
-    conv = wide[first : first + rows, :] * taps[0:1, :].astype(jnp.float32)
-    for j in range(1, tap_count):
-        conv = conv + wide[first + j : first + j + rows, :] * taps[j : j + 1, :].astype(jnp.float32)
-    conv = conv.astype(jnp.bfloat16)
-    to_recur = jnp.dot(conv, wr[0], preferred_element_type=jnp.float32)
-    to_input = jnp.dot(conv, wi[0], preferred_element_type=jnp.float32)
-    gate_recur = 0.5 * jnp.tanh(0.5 * to_recur) + 0.5
-    gate_input = 0.5 * jnp.tanh(0.5 * to_input) + 0.5
+    tap = [taps[j : j + 1, :].astype(jnp.float32) for j in range(tap_count)]
+    step_rows = 64 if rows % 64 == 0 else rows
+    for i in range(rows // step_rows):
+        low = i * step_rows
+        conv = wide[first + low : first + low + step_rows, :] * tap[0]
+        for j in range(1, tap_count):
+            conv = conv + wide[first + low + j : first + low + j + step_rows, :] * tap[j]
+        conv_at[low : low + step_rows, :] = conv.astype(jnp.bfloat16)
+    to_recur[...] = jnp.dot(conv_at[...], wr[0], preferred_element_type=jnp.float32)
+    to_input[...] = jnp.dot(conv_at[...], wi[0], preferred_element_type=jnp.float32)
     rate = jnp.exp(rate_log[...]) * (-RECUR_SCALE / length)
-    log_decay = gate_recur * rate + shift[0]
-    decay = jnp.exp(log_decay)
-    twice = 2.0 * log_decay
-    series = 1.0 + twice * (1.0 / 8.0)
-    for k in range(7, 1, -1):
-        series = 1.0 + twice * (1.0 / k) * series
-    gone = jnp.where(twice > -0.5, -twice * series, 1.0 - decay * decay)
-    root = gone * lax.rsqrt(jnp.maximum(gone, 1e-37))
-    drive = root * gate_input * conv.astype(jnp.float32)
-    width = wide.shape[1]
-    lanes = [slice(b * LANES, (b + 1) * LANES) for b in range(width // LANES)]
+    half_rate = 0.5 * rate
     for b, cols in enumerate(lanes):
-        p_out[0, b] = decay[:, cols]
-        h_out[0, b] = drive[:, cols]
+
+        def gates(i, _, b=b, cols=cols):
+            at = pl.ds(pl.multiple_of(i * step_rows, step_rows), step_rows)
+            log_decay = jnp.tanh(0.5 * to_recur[at, cols]) * half_rate[:, cols] + (
+                half_rate[:, cols] + shift[0, at, cols]
+            )
+            decay = jnp.exp(log_decay)
+            gone = jnp.tanh(-log_decay) * (1.0 + decay * decay)
+            root = gone * lax.rsqrt(jnp.maximum(gone, 1e-37))
+            gate_input = 0.5 * jnp.tanh(0.5 * to_input[at, cols]) + 0.5
+            p_out[0, b, at, :] = decay
+            h_out[0, b, at, :] = root * gate_input * conv_at[at, cols].astype(jnp.float32)
+            return 0
+
+        lax.fori_loop(0, rows // step_rows, gates, 0, unroll=2)
     states = [jnp.zeros((CHUNKS, LANES), jnp.float32) for _ in lanes]
     keeps = [jnp.ones((CHUNKS, LANES), jnp.float32) for _ in lanes]
     for t in range(span):
@@ -237,8 +259,8 @@
     return pl.pallas_call(
         functools.partial(chain_kernel, length),
         out_shape=(
-            jax.ShapeDtypeStruct((seqs, width // LANES, rows, LANES), jnp.float32),
-            jax.ShapeDtypeStruct((seqs, width // LANES, rows, LANES), jnp.float32),
+            pltpu.HBM((seqs, width // LANES, rows, LANES), jnp.float32),
+            pltpu.HBM((seqs, width // LANES, rows, LANES), jnp.float32),
             jax.ShapeDtypeStruct((seqs, 2 * CHUNKS, width), jnp.float32),
             jax.ShapeDtypeStruct((seqs, 2 * CHUNKS, width), jnp.float32),
         ),
@@ -257,8 +279,13 @@
             pl.BlockSpec((1, 2 * CHUNKS, head), lambda i, g: (i, 0, g)),
             pl.BlockSpec((1, 2 * CHUNKS, head), lambda i, g: (i, 0, g)),
         ),
-        scratch_shapes=[pltpu.VMEM((rows + HALO, head), jnp.float32)],
-        compiler_params=pltpu.CompilerParams(vmem_limit_bytes=24 * MIB),
+        scratch_shapes=[
+            pltpu.VMEM((rows + HALO, head), jnp.float32),
+            pltpu.VMEM((rows, head), jnp.bfloat16),
+            pltpu.VMEM((rows, head), jnp.float32),
+            pltpu.VMEM((rows, head), jnp.float32),
+        ],
+        compiler_params=pltpu.CompilerParams(vmem_limit_bytes=10 * MIB),
         cost_estimate=pl.CostEstimate(
             flops=8_000_000_000, transcendentals=0, bytes_accessed=12_000_000
         ),
@@ -320,7 +347,7 @@
                 pltpu.VMEM((3, 8 + total, head), jnp.float32),
             ],
         ),
-        compiler_params=pltpu.CompilerParams(vmem_limit_bytes=24 * MIB),
+        compiler_params=pltpu.CompilerParams(vmem_limit_bytes=8 * MIB),
         cost_estimate=pl.CostEstimate(
             flops=4_000_000_000, transcendentals=0, bytes_accessed=4_000_000
         ),
@@ -329,31 +356,40 @@
 
 
 def recurrent_kernel(h, p, seam_h, seam_p, entering, out):
-    seqs, blocks, rows, _ = h.shape
+    _, blocks, rows, _ = h.shape
     span = rows // CHUNKS
-    for s in range(seqs):
-        for b in range(blocks):
-            cols = slice(b * LANES, (b + 1) * LANES)
-            for c in range(CHUNKS):
-                one = slice(c, c + 1)
-                gone_in = seam_h[s, one, cols] + seam_p[s, one, cols] * entering[s : s + 1, cols]
-                at = slice(c * span, (c + 1) * span)
-                out[s, at, cols] = (h[s, b, at, :] + p[s, b, at, :] * gone_in).astype(out.dtype)
+    for b in range(blocks):
+        cols = slice(b * LANES, (b + 1) * LANES)
+        for c in range(CHUNKS):
+            one = slice(c, c + 1)
+            gone_in = seam_h[0, one, cols] + seam_p[0, one, cols] * entering[0, 0:1, cols]
+            at = slice(c * span, (c + 1) * span)
+            out[0, at, cols] = (h[0, b, at, :] + p[0, b, at, :] * gone_in).astype(out.dtype)
 
 
 def recurrent_rows(h, p, seam_h, seam_p, entering):
     seqs, blocks, rows, _ = h.shape
-    vmem = pl.BlockSpec(memory_space=pltpu.VMEM)
+    width = blocks * LANES
+    group = 2
+    block = pl.BlockSpec((1, group, rows, LANES), lambda i, g: (i, g, 0, 0))
+    seam = pl.BlockSpec((1, 2 * CHUNKS, group * LANES), lambda i, g: (i, 0, g))
     return pl.pallas_call(
         recurrent_kernel,
-        out_shape=jax.ShapeDtypeStruct((seqs, rows, blocks * LANES), jnp.bfloat16),
-        in_specs=[vmem] * 5,
-        out_specs=vmem,
-        compiler_params=pltpu.CompilerParams(vmem_limit_bytes=16 * MIB),
+        out_shape=jax.ShapeDtypeStruct((seqs, rows, width), jnp.bfloat16),
+        grid=(seqs, blocks // group),
+        in_specs=[
+            block,
+            block,
+            seam,
+            seam,
+            pl.BlockSpec((1, 1, group * LANES), lambda i, g: (i, 0, g)),
+        ],
+        out_specs=pl.BlockSpec((1, rows, group * LANES), lambda i, g: (i, 0, g)),
+        compiler_params=pltpu.CompilerParams(vmem_limit_bytes=8 * MIB),
         cost_estimate=pl.CostEstimate(
             flops=2_000_000_000, transcendentals=0, bytes_accessed=8_000_000
         ),
-    )(h, p, seam_h, seam_p, entering)
+    )(h, p, seam_h, seam_p, entering[:, None])
 
 
 def exit_kernel(chain_spots, pool_spots, counts, shards, merged, *refs):
@@ -452,7 +488,7 @@
         functools.partial(exit_kernel, chain_spots, pool_spots, counts, shards, merge is not None),
         out_shape=out_shape,
         in_specs=specs,
-        compiler_params=pltpu.CompilerParams(vmem_limit_bytes=32 * MIB),
+        compiler_params=pltpu.CompilerParams(vmem_limit_bytes=18 * MIB),
         cost_estimate=pl.CostEstimate(
             flops=4 * seqs * half * width * wide, transcendentals=0, bytes_accessed=6_000_000
         ),
@@ -515,8 +551,9 @@
     swap_tp = [(0, 1), (1, 0)]
     other = lax.ppermute(tokens, "tp", swap_tp)
     tail = jnp.where(core == 1, tokens[:, half - HALO :], other[:, half - HALO :])
-    halo = lax.ppermute(tail, "sp", [(i, i + 1) for i in range(sp_n - 1)])
-    normed = norm_rows(order, side, tokens, other, halo, norm_gain)
+    halo = lax.ppermute(tail, "sp", ring_pairs(sp_n))
+    spot = jnp.stack([core, place]).astype(jnp.int32)
+    normed = norm_rows(order, spot, tokens, other, halo, norm_gain)
 
     chain_input = entry_dot(normed, ce)
     pool_input = entry_dot(normed, pe)
@@ -527,7 +564,7 @@
     last = jnp.stack([seam_p[:, CHUNKS], seam_h[:, CHUNKS]])
     entering = start_state
     for back in range(sp_n - 1, 0, -1):
-        came = lax.ppermute(last, "sp", [(i, i + back) for i in range(sp_n - back)])
+        came = lax.ppermute(last, "sp", [(i, (i + back) % sp_n) for i in range(sp_n)])
         entering = jnp.where(place >= back, came[0] * entering + came[1], entering)
 
     start = jnp.reshape(place * rows, (1,)).astype(jnp.int32)

time: 171 us -> 171 us (level)
  the two profiles are of different devices: /device:TPU:1 before, /device:TPU:11 now
where the time goes in v1:
time: 171 us; the launch traced here: 170 us
  waiting for transfers between devices  67.1 us (39%)
  starting transfers between devices  58.2 us (34%)
  Pallas kernels  40.2 us (24%)
  other arithmetic  3.27 us (2%)
    ppermute x34, waiting for transfers between devices, swapped(): came = lax.ppermute(stack, 'fs', swap_pairs(fs_n, bit))  31.5 us
    ppermute x34, starting transfers between devices, swapped(): came = lax.ppermute(stack, 'fs', swap_pairs(fs_n, bit))  23.8 us
    ppermute x3, waiting for transfers between devices, per_device(): lax.ppermute(last, 'sp', [(i, (i + back) % sp_n) for i in range(sp_n)])  17.2 us
    pallas_call x2, Pallas kernels, entry_dot(): pl.pallas_call(functools.partial(entry_kernel, [places for _, places in p...  11.5 us
    pallas_call x1, Pallas kernels, chain_scan(): pl.pallas_call(functools.partial(chain_kernel, length), out_shape=(pltpu....  11.5 us
    ppermute x6, waiting for transfers between devices, gather_part(): held = (lax.ppermute(past[0][0], 'sp', ring), [(0, lap)])  10.1 us
    pallas_call x4, Pallas kernels, exit_columns(): pl.pallas_call(functools.partial(exit_kernel, chain_spots, pool_spots, co...  9.98 us
    ppermute x1, starting transfers between devices, per_device(): came_early = lax.ppermute(ex(other_side, early), 'tp', swap_tp)  8.6 us
  transfers between devices with their start and end apart: 53, of which 22 were waited for; matrix products, arithmetic and copies ran while one was open for 2% of the time, Pallas kernels for 22%

profile of v1, /device:TPU:11, one launch (start us, length us, event | category | flops | bytes accessed | tf_op | source)
XLA Modules:
  0.0 170.3 jit_solution(14272389262758257649)
XLA Ops:
  0.7 1.3 collective-permute-start.5
  2.0 1.2 collective-permute-start.3
  3.5 1.3 collective-permute-start.23
  4.8 4.0 %collective-permute-done.5.refs_4_ = bf16[1,128,1024]{2,1,0:T(8,128)(2,1)} collective-permute-done((bf16[1,128,1024]{2,1,0:T(8,128)(2,1)}, bf16[1,128,1024]{2,1,0:T(8,128)(2,1)}, u32[]{:S(2)}, u32[]{:S(2)}) %collective-permute-start.5) | collective-permute-done | bytes 262176 | tf_op jit(solution)/shard_map/ppermute | solution.py:57
  8.8 1.2 collective-permute-start.21
  12.0 2.4 %collective-permute-done.23.refs_4_ = bf16[1,128,1024]{2,1,0:T(8,128)(2,1)S(1)} collective-permute-done((bf16[1,128,1024]{2,1,0:T(8,128)(2,1)}, bf16[1,128,1024]{2,1,0:T(8,128)(2,1)S(1)}, u32[]{:S(2)}, u32[]{:S(2)}) %collective-permute-start.23) | collective-permute-done | bytes 262176 | tf_op jit(solution)/shard_map/ppermute | solution.py:57
  14.4 1.3 collective-permute-start.9
  17.3 3.9 %collective-permute-done.35 = bf16[1,1024,128]{2,1,0:T(8,128)(2,1)} collective-permute-done((bf16[1,1024,128]{2,1,0:T(8,128)(2,1)}, bf16[1,1024,128]{2,1,0:T(8,128)(2,1)}, u32[]{:S(2)}, u32[]{:S(2)}) %collective-permute-start.35) | collective-permute-done | bytes 262176 | tf_op jit(solution)/shard_map/ppermute | solution.py:40
  21.2 1.2 collective-permute-start.7
  22.5 1.2 collective-permute-start.13
  23.9 1.3 collective-permute-start.27
  25.9 1.1 collective-permute-done.7.refs_6_
  27.3 3.5 %collective-permute-done.13.refs_12_ = bf16[1,128,1024]{2,1,0:T(8,128)(2,1)} collective-permute-done((bf16[1,128,1024]{2,1,0:T(8,128)(2,1)}, bf16[1,128,1024]{2,1,0:T(8,128)(2,1)}, u32[]{:S(2)}, u32[]{:S(2)}) %collective-permute-start.13) | collective-permute-done | bytes 262176 | tf_op jit(solution)/shard_map/ppermute | solution.py:57
  30.8 1.2 collective-permute-start.11
  33.2 2.7 %collective-permute-done.4.refs_3_ = bf16[1,128,1024]{2,1,0:T(8,128)(2,1)S(1)} collective-permute-done((bf16[1,128,1024]{2,1,0:T(8,128)(2,1)}, bf16[1,128,1024]{2,1,0:T(8,128)(2,1)S(1)}, u32[]{:S(2)}, u32[]{:S(2)}) %collective-permute-start.4) | collective-permute-done | bytes 262176 | tf_op jit(solution)/shard_map/ppermute | solution.py:40
  35.9 2.5 %collective-permute-start.1 = (bf16[2,16,2048]{2,1,0:T(8,128)(2,1)S(1)}, bf16[2,16,2048]{2,1,0:T(8,128)(2,1)S(1)}, u32[]{:S(2)}, u32[]{:S(2)}) collective-permute-start(bf16[2,16,2048]{2,1,0:T(8,128)(2,1)S(1)} %slice_select_fusion), channel_id=1, source_target_pairs={{0,8},{8,16},{16,24},{24,0},{1,9},{9,17},{17,25},{25,1},{2,10},{10... | collective-permute-start | bytes 393224 | tf_op jit(solution)/shard_map/ppermute | solution.py:554
  38.4 1.1 pad_maximum_fusion.refs_3_.refs_5_
  39.5 1.1 pad_maximum_fusion.1.refs_9_.refs_11_
  43.6 1.2 collective-permute-start.16
  44.9 2.9 %norm_rows.1 = bf16[2,400,2048]{2,1,0:T(8,128)(2,1)S(1)} custom-call(s32[16]{0:T(128)S(1)} %add.41.order.refs_0_, s32[2]{0:T(128)S(1)} %pad_add_fusion.spot, bf16[2,192,2048]{2,1,0:T(8,128)(2,1)S(1)} %copy-done.2, bf16[2,192,2048]{2,1,0:T(8,128)(2,1)S(1)} %collective-permute-done.other, bf16[2,16,2048]{2,1,0:T(8,128)(2,1)S(1)} %collective-permute-done.1.halo, ...), custom_call_target="tpu_custom_call" | custom-call | flops 4000000000 | bytes 8000000 | tf_op jit(solution)/shard_map/norm_rows/pallas_call | solution.py:123
  47.8 1.4 collective-permute-done.10.refs_9_
  49.2 1.2 collective-permute-start.25
  50.7 1.0 collective-permute-start.31
  52.6 1.2 collective-permute-start.29
  54.1 5.9 %shard_map.136 = bf16[800,1024]{1,0:T(8,128)(2,1)S(1)} custom-call(bf16[800,2048]{1,0:T(8,128)(2,1)S(1)} %bitcast.76, bf16[1,128,1024]{2,1,0:T(8,128)(2,1)S(1)} %bitcast.68, bf16[1,128,1024]{2,1,0:T(8,128)(2,1)S(1)} %copy-done.10, bf16[1,128,1024]{2,1,0:T(8,128)(2,1)} %collective-permute-done.3.refs_2_, ...), custom_call_target="tpu_custom_call" | custom-call | flops 3355443200 | bytes 4194304 | tf_op jit(solution)/shard_map/pallas_call | solution.py:178
  61.0 1.2 collective-permute-start.46
  62.2 1.8 %collective-permute-start.41 = (bf16[2,1024,128]{2,1,0:T(8,128)(2,1)S(1)}, bf16[2,1024,128]{2,1,0:T(8,128)(2,1)S(1)}, u32[]{:S(2)}, u32[]{:S(2)}) collective-permute-start(bf16[2,1024,128]{2,1,0:T(8,128)(2,1)S(1)} %pad_maximum_fusion.1.refs_9_.refs_11_), channel_id=1, source_target_pairs={{0,8},{8,16},{16,24},{24,0},{1,9},{9,17},{17,25},{25,1},{2,10},{10... | collective-permute-start | bytes 1572872 | tf_op jit(solution)/shard_map/ppermute | solution.py:80
  64.2 1.2 collective-permute-start.32
  65.4 11.5 %chain_scan.1 = (f32[2,8,384,128]{3,2,1,0:T(8,128)}, f32[2,8,384,128]{3,2,1,0:T(8,128)}, f32[2,16,1024]{2,1,0:T(8,128)S(1)}, f32[2,16,1024]{2,1,0:T(8,128)S(1)}) custom-call(bf16[2,400,1024]{2,1,0:T(8,128)(2,1)S(1)} %bitcast.78, bf16[4,1024]{1,0:T(4,128)(2,1)S(1)} %copy-done.12, bf16[4,256,256]{2,1,0:T(8,128)(2,1)S(1)} %copy-done.4, ...), custom_call_target="tpu_custom_call" | custom-call | flops 8000000000 | bytes 12000000 | tf_op jit(solution)/shard_map/chain_scan/pallas_call | solution.py:259
  77.6 1.4 collective-permute-start.30
  79.0 1.3 collective-permute-start.37
  81.1 1.6 collective-permute-done.33.refs_14_
  82.8 3.8 %collective-permute-start.17 = (f32[2,2,1024]{2,1,0:T(2,128)S(1)}, f32[2,2,1024]{2,1,0:T(2,128)S(1)}, u32[]{:S(2)}, u32[]{:S(2)}) collective-permute-start(f32[2,2,1024]{2,1,0:T(2,128)S(1)} %pad_maximum_fusion.2), channel_id=1, source_target_pairs={{0,8},{8,16},{16,24},{24,0},{1,9},{9,17},{17,25},{25,1},{2,10},{10... | collective-permute-start | bytes 49160 | tf_op jit(solution)/shard_map/ppermute | solution.py:567
  86.6 2.6 %collective-permute-start.18 = (f32[2,2,1024]{2,1,0:T(2,128)S(1)}, f32[2,2,1024]{2,1,0:T(2,128)S(1)}, u32[]{:S(2)}, u32[]{:S(2)}) collective-permute-start(f32[2,2,1024]{2,1,0:T(2,128)S(1)} %pad_maximum_fusion.2), channel_id=1, source_target_pairs={{0,16},{8,24},{16,0},{24,8},{1,17},{9,25},{17,1},{25,9},{2,18},{10... | collective-permute-start | bytes 49160 | tf_op jit(solution)/shard_map/ppermute | solution.py:567
  89.9 5.6 %shard_map.138 = bf16[800,1024]{1,0:T(8,128)(2,1)S(1)} custom-call(bf16[800,2048]{1,0:T(8,128)(2,1)S(1)} %bitcast.77, bf16[1,128,1024]{2,1,0:T(8,128)(2,1)S(1)} %bitcast.72, bf16[1,128,1024]{2,1,0:T(8,128)(2,1)} %collective-permute-done.20.refs_1_, bf16[1,128,1024]{2,1,0:T(8,128)(2,1)} %collective-permute-done.21.refs_2_, ...), custom_call_target="tpu_custom_call" | custom-call | flops 3355443200 | bytes 4194304 | tf_op jit(solution)/shard_map/pallas_call | solution.py:178
  96.0 5.1 %collective-permute-done.42.refs_13_.refs_15_ = bf16[2,1024,128]{2,1,0:T(8,128)(2,1)S(1)} collective-permute-done((bf16[2,1024,128]{2,1,0:T(8,128)(2,1)S(1)}, bf16[2,1024,128]{2,1,0:T(8,128)(2,1)S(1)}, u32[]{:S(2)}, u32[]{:S(2)}) %collective-permute-start.42) | collective-permute-done | bytes 524320 | tf_op jit(solution)/shard_map/ppermute | solution.py:80
  103.4 16.7 %collective-permute-done.19 = f32[2,2,1024]{2,1,0:T(2,128)S(1)} collective-permute-done((f32[2,2,1024]{2,1,0:T(2,128)S(1)}, f32[2,2,1024]{2,1,0:T(2,128)S(1)}, u32[]{:S(2)}, u32[]{:S(2)}) %collective-permute-start.19) | collective-permute-done | bytes 16416 | tf_op jit(solution)/shard_map/ppermute | solution.py:567
  120.1 1.5 collective-permute-start.51
  121.6 3.3 %pool_mixed.1.refs_2_.refs_3_ = bf16[2,384,1024]{2,1,0:T(8,128)(2,1)S(1)} custom-call(s32[1]{0:T(128)} %bitcast.15.start, bf16[2,400,1024]{2,1,0:T(8,128)(2,1)S(1)} %bitcast.79, bf16[4,256,256]{2,1,0:T(8,128)(2,1)S(1)} %copy-done.6, f32[1,1024]{1,0:T(1,128)S(1)} %bitcast.75), custom_call_target="tpu_custom_call" | custom-call | flops 4000000000 | bytes 4000000 | tf_op jit(solution)/shard_map/pool_mixed/pallas_call | solution.py:333
  126.0 8.0 %collective-permute-done.51.refs_14_.refs_16_ = bf16[2,1024,128]{2,1,0:T(8,128)(2,1)S(1)} collective-permute-done((bf16[2,1024,128]{2,1,0:T(8,128)(2,1)S(1)}, bf16[2,1024,128]{2,1,0:T(8,128)(2,1)S(1)}, u32[]{:S(2)}, u32[]{:S(2)}) %collective-permute-start.51) | collective-permute-done | bytes 524320 | tf_op jit(solution)/shard_map/ppermute | solution.py:40
  134.0 2.6 %shard_map.140 = bf16[2,192,1536]{2,1,0:T(8,128)(2,1)S(1)} custom-call(s32[1]{0:T(128)S(6)} %sub.16.refs_0_, bf16[2,384,1024]{2,1,0:T(8,128)(2,1)S(1)} %shard_map.137.refs_1_.refs_2_, bf16[2,384,1024]{2,1,0:T(8,128)(2,1)S(1)} %pool_mixed.1.refs_2_.refs_3_, bf16[2,1024,128]{2,1,0:T(8,128)(2,1)S(1)} %pad_maximum_fusion.refs_3_.refs_5_, ...), custom_call_target="tpu_custom_call" | custom-call | flops 2415919104 | bytes 6000000 | tf_op jit(solution)/shard_map/pallas_call | solution.py:487
  136.6 8.6 %collective-permute-start.52 = (bf16[2,192,1536]{2,1,0:T(8,128)(2,1)S(1)}, bf16[2,192,1536]{2,1,0:T(8,128)(2,1)S(1)}, u32[]{:S(2)}, u32[]{:S(2)}) collective-permute-start(bf16[2,192,1536]{2,1,0:T(8,128)(2,1)S(1)} %shard_map.140), channel_id=1, source_target_pairs={{0,1},{1,0},{2,3},{3,2},{4,5},{5,4},{6,7},{7,6},{8,9},{9,8},{10,11... | collective-permute-start | bytes 3538952 | tf_op jit(solution)/shard_map/ppermute | solution.py:580
  145.2 3.1 %collective-permute-done.43.refs_5_.refs_7_ = bf16[2,1024,128]{2,1,0:T(8,128)(2,1)S(1)} collective-permute-done((bf16[2,1024,128]{2,1,0:T(8,128)(2,1)S(1)}, bf16[2,1024,128]{2,1,0:T(8,128)(2,1)S(1)}, u32[]{:S(2)}, u32[]{:S(2)}) %collective-permute-start.43) | collective-permute-done | bytes 524320 | tf_op jit(solution)/shard_map/ppermute | solution.py:80
  148.4 10.2 %collective-permute-done.39.refs_4_.refs_6_ = bf16[2,1024,128]{2,1,0:T(8,128)(2,1)S(1)} collective-permute-done((bf16[2,1024,128]{2,1,0:T(8,128)(2,1)S(1)}, bf16[2,1024,128]{2,1,0:T(8,128)(2,1)S(1)}, u32[]{:S(2)}, u32[]{:S(2)}) %collective-permute-start.39) | collective-permute-done | bytes 524320 | tf_op jit(solution)/shard_map/ppermute | solution.py:40
  158.7 1.0 shard_map.139
  159.7 4.0 %collective-permute-start.45 = (bf16[2,192,512]{2,1,0:T(8,128)(2,1)S(1)}, bf16[2,192,512]{2,1,0:T(8,128)(2,1)S(1)}, u32[]{:S(2)}, u32[]{:S(2)}) collective-permute-start(bf16[2,192,512]{2,1,0:T(8,128)(2,1)S(1)} %shard_map.139), channel_id=1, source_target_pairs={{0,1},{1,0},{2,3},{3,2},{4,5},{5,4},{6,7},{7,6},{8,9},{9,8},{10,11... | collective-permute-start | bytes 1179656 | tf_op jit(solution)/shard_map/ppermute | solution.py:581
  163.8 4.1 %shard_map.141.refs_9_ = bf16[2,192,2048]{2,1,0:T(8,128)(2,1)} custom-call(s32[16]{0:T(128)S(1)} %add.41.order.refs_0_, s32[1]{0:T(128)} %bitcast.refs_1_, bf16[2,384,1024]{2,1,0:T(8,128)(2,1)S(1)} %shard_map.137.refs_1_.refs_2_, bf16[2,384,1024]{2,1,0:T(8,128)(2,1)S(1)} %pool_mixed.1.refs_2_.refs_3_, ...), custom_call_target="tpu_custom_call" | custom-call | flops 2415919104 | bytes 6000000 | tf_op jit(solution)/shard_map/pallas_call | solution.py:487
  167.9 2.3 %shard_map.142 = bf16[2,192,2048]{2,1,0:T(8,128)(2,1)} custom-call(s32[16]{0:T(128)S(1)} %add.41.order.refs_0_, s32[1]{0:T(128)} %bitcast.refs_1_, bf16[2,384,1024]{2,1,0:T(8,128)(2,1)S(1)} %shard_map.137.refs_1_.refs_2_, bf16[2,384,1024]{2,1,0:T(8,128)(2,1)S(1)} %pool_mixed.1.refs_2_.refs_3_, ...), custom_call_target="tpu_custom_call", output_to_operand_aliasing={{}: (9, {})} | custom-call | flops 805306368 | bytes 6000000 | tf_op jit(solution)/shard_map/pallas_call | solution.py:487
  (114 shorter events, 18.7 us)
Async XLA Ops:
  0.0 32.1 %collective-permute-start = (bf16[2,192,2048]{2,1,0:T(8,128)(2,1)}, bf16[2,192,2048]{2,1,0:T(8,128)(2,1)S(1)}, u32[]{:S(2)}, u32[]{:S(2)}) collective-permute-start(bf16[2,192,2048]{2,1,0:T(8,128)(2,1)} %own.1), channel_id=1, source_target_pairs={{0,1},{1,0},{2,3},{3,2},{4,5},{5,4},{6,7},{7,6},{8,9},{9,8},{10,11... | collective-permute-start | bytes 4718600 | tf_op jit(solution)/shard_map/ppermute | solution.py:552
  0.7 8.1 %collective-permute-start.5 = (bf16[1,128,1024]{2,1,0:T(8,128)(2,1)}, bf16[1,128,1024]{2,1,0:T(8,128)(2,1)}, u32[]{:S(2)}, u32[]{:S(2)}) collective-permute-start(bf16[1,128,1024]{2,1,0:T(8,128)(2,1)} %bitcast.65), channel_id=1, source_target_pairs={{0,8},{8,16},{16,24},{24,0},{1,9},{9,17},{17,25},{25,1},{2,10},{10... | collective-permute-start | bytes 786440 | tf_op jit(solution)/shard_map/ppermute | solution.py:57
  2.0 8.1 %collective-permute-start.3 = (bf16[1,128,1024]{2,1,0:T(8,128)(2,1)}, bf16[1,128,1024]{2,1,0:T(8,128)(2,1)}, u32[]{:S(2)}, u32[]{:S(2)}) collective-permute-start(bf16[1,128,1024]{2,1,0:T(8,128)(2,1)} %bitcast.66), channel_id=1, source_target_pairs={{0,4},{2,6},{4,0},{6,2},{1,5},{3,7},{5,1},{7,3},{8,12},{10,14},{12... | collective-permute-start | bytes 786440 | tf_op jit(solution)/shard_map/ppermute | solution.py:40
  3.5 10.9 %collective-permute-start.23 = (bf16[1,128,1024]{2,1,0:T(8,128)(2,1)}, bf16[1,128,1024]{2,1,0:T(8,128)(2,1)S(1)}, u32[]{:S(2)}, u32[]{:S(2)}) collective-permute-start(bf16[1,128,1024]{2,1,0:T(8,128)(2,1)} %bitcast.69), channel_id=1, source_target_pairs={{0,8},{8,16},{16,24},{24,0},{1,9},{9,17},{17,25},{25,1},{2,10},{10... | collective-permute-start | bytes 786440 | tf_op jit(solution)/shard_map/ppermute | solution.py:57
  11.4 9.8 %collective-permute-start.35 = (bf16[1,1024,128]{2,1,0:T(8,128)(2,1)}, bf16[1,1024,128]{2,1,0:T(8,128)(2,1)}, u32[]{:S(2)}, u32[]{:S(2)}) collective-permute-start(bf16[1,1024,128]{2,1,0:T(8,128)(2,1)} %bitcast.80), channel_id=1, source_target_pairs={{0,4},{2,6},{4,0},{6,2},{1,5},{3,7},{5,1},{7,3},{8,12},{10,14},{12... | collective-permute-start | bytes 786440 | tf_op jit(solution)/shard_map/ppermute | solution.py:40
  14.4 8.1 %collective-permute-start.9 = (bf16[1,128,1024]{2,1,0:T(8,128)(2,1)}, bf16[1,128,1024]{2,1,0:T(8,128)(2,1)}, u32[]{:S(2)}, u32[]{:S(2)}) collective-permute-start(bf16[1,128,1024]{2,1,0:T(8,128)(2,1)} %collective-permute-done.5.refs_4_), channel_id=1, source_target_pairs={{0,8},{8,16},{16,24},{24,0},{1,9},{9,17},{17,25},{25,1},{2,10},{10... | collective-permute-start | bytes 786440 | tf_op jit(solution)/shard_map/ppermute | solution.py:57
  15.7 8.2 %collective-permute-start.40 = (bf16[1,1024,128]{2,1,0:T(8,128)(2,1)}, bf16[1,1024,128]{2,1,0:T(8,128)(2,1)}, u32[]{:S(2)}, u32[]{:S(2)}) collective-permute-start(bf16[1,1024,128]{2,1,0:T(8,128)(2,1)} %bitcast.82), channel_id=1, source_target_pairs={{0,2},{2,0},{4,6},{6,4},{1,3},{3,1},{5,7},{7,5},{8,10},{10,8},{12,... | collective-permute-start | bytes 786440 | tf_op jit(solution)/shard_map/ppermute | solution.py:40
  16.5 9.1 %collective-permute-start.6 = (bf16[1,128,1024]{2,1,0:T(8,128)(2,1)}, bf16[1,128,1024]{2,1,0:T(8,128)(2,1)}, u32[]{:S(2)}, u32[]{:S(2)}) collective-permute-start(bf16[1,128,1024]{2,1,0:T(8,128)(2,1)} %collective-permute-done.5.refs_4_), channel_id=1, source_target_pairs={{0,2},{2,0},{4,6},{6,4},{1,3},{3,1},{5,7},{7,5},{8,10},{10,8},{12,... | collective-permute-start | bytes 786440 | tf_op jit(solution)/shard_map/ppermute | solution.py:40
  22.5 8.3 %collective-permute-start.13 = (bf16[1,128,1024]{2,1,0:T(8,128)(2,1)}, bf16[1,128,1024]{2,1,0:T(8,128)(2,1)}, u32[]{:S(2)}, u32[]{:S(2)}) collective-permute-start(bf16[1,128,1024]{2,1,0:T(8,128)(2,1)} %collective-permute-done.9.refs_8_), channel_id=1, source_target_pairs={{0,8},{8,16},{16,24},{24,0},{1,9},{9,17},{17,25},{25,1},{2,10},{10... | collective-permute-start | bytes 786440 | tf_op jit(solution)/shard_map/ppermute | solution.py:57
  23.9 16.6 %collective-permute-start.27 = (bf16[1,128,1024]{2,1,0:T(8,128)(2,1)S(1)}, bf16[1,128,1024]{2,1,0:T(8,128)(2,1)S(1)}, u32[]{:S(2)}, u32[]{:S(2)}) collective-permute-start(bf16[1,128,1024]{2,1,0:T(8,128)(2,1)S(1)} %collective-permute-done.23.refs_4_), channel_id=1, source_target_pairs={{0,8},{8,16},{16,24},{24,0},{1,9},{9,17},{17,25},{25,1},{2,10},{10... | collective-permute-start | bytes 786440 | tf_op jit(solution)/shard_map/ppermute | solution.py:57
  25.7 15.7 %collective-permute-start.24 = (bf16[1,128,1024]{2,1,0:T(8,128)(2,1)S(1)}, bf16[1,128,1024]{2,1,0:T(8,128)(2,1)S(1)}, u32[]{:S(2)}, u32[]{:S(2)}) collective-permute-start(bf16[1,128,1024]{2,1,0:T(8,128)(2,1)S(1)} %collective-permute-done.23.refs_4_), channel_id=1, source_target_pairs={{0,2},{2,0},{4,6},{6,4},{1,3},{3,1},{5,7},{7,5},{8,10},{10,8},{12,... | collective-permute-start | bytes 786440 | tf_op jit(solution)/shard_map/ppermute | solution.py:40
  27.1 8.9 %collective-permute-start.4 = (bf16[1,128,1024]{2,1,0:T(8,128)(2,1)}, bf16[1,128,1024]{2,1,0:T(8,128)(2,1)S(1)}, u32[]{:S(2)}, u32[]{:S(2)}) collective-permute-start(bf16[1,128,1024]{2,1,0:T(8,128)(2,1)} %collective-permute-done.3.refs_2_), channel_id=1, source_target_pairs={{0,2},{2,0},{4,6},{6,4},{1,3},{3,1},{5,7},{7,5},{8,10},{10,8},{12,... | collective-permute-start | bytes 786440 | tf_op jit(solution)/shard_map/ppermute | solution.py:40
  30.8 11.3 %collective-permute-start.11 = (bf16[1,128,1024]{2,1,0:T(8,128)(2,1)}, bf16[1,128,1024]{2,1,0:T(8,128)(2,1)S(1)}, u32[]{:S(2)}, u32[]{:S(2)}) collective-permute-start(bf16[1,128,1024]{2,1,0:T(8,128)(2,1)} %collective-permute-done.9.refs_8_), channel_id=1, source_target_pairs={{0,4},{2,6},{4,0},{6,2},{1,5},{3,7},{5,1},{7,3},{8,12},{10,14},{12... | collective-permute-start | bytes 786440 | tf_op jit(solution)/shard_map/ppermute | solution.py:40
  32.1 10.8 %collective-permute-start.14 = (bf16[1,128,1024]{2,1,0:T(8,128)(2,1)}, bf16[1,128,1024]{2,1,0:T(8,128)(2,1)S(1)}, u32[]{:S(2)}, u32[]{:S(2)}) collective-permute-start(bf16[1,128,1024]{2,1,0:T(8,128)(2,1)} %collective-permute-done.13.refs_12_), channel_id=1, source_target_pairs={{0,2},{2,0},{4,6},{6,4},{1,3},{3,1},{5,7},{7,5},{8,10},{10,8},{12,... | collective-permute-start | bytes 786440 | tf_op jit(solution)/shard_map/ppermute | solution.py:40
  35.9 7.7 %collective-permute-start.1 = (bf16[2,16,2048]{2,1,0:T(8,128)(2,1)S(1)}, bf16[2,16,2048]{2,1,0:T(8,128)(2,1)S(1)}, u32[]{:S(2)}, u32[]{:S(2)}) collective-permute-start(bf16[2,16,2048]{2,1,0:T(8,128)(2,1)S(1)} %slice_select_fusion), channel_id=1, source_target_pairs={{0,8},{8,16},{16,24},{24,0},{1,9},{9,17},{17,25},{25,1},{2,10},{10... | collective-permute-start | bytes 393224 | tf_op jit(solution)/shard_map/ppermute | solution.py:554
  40.6 8.6 %collective-permute-start.10 = (bf16[1,128,1024]{2,1,0:T(8,128)(2,1)}, bf16[1,128,1024]{2,1,0:T(8,128)(2,1)S(1)}, u32[]{:S(2)}, u32[]{:S(2)}) collective-permute-start(bf16[1,128,1024]{2,1,0:T(8,128)(2,1)} %collective-permute-done.9.refs_8_), channel_id=1, source_target_pairs={{0,2},{2,0},{4,6},{6,4},{1,3},{3,1},{5,7},{7,5},{8,10},{10,8},{12,... | collective-permute-start | bytes 786440 | tf_op jit(solution)/shard_map/ppermute | solution.py:40
  41.4 9.1 %collective-permute-start.8 = (bf16[1,128,1024]{2,1,0:T(8,128)(2,1)}, bf16[1,128,1024]{2,1,0:T(8,128)(2,1)S(1)}, u32[]{:S(2)}, u32[]{:S(2)}) collective-permute-start(bf16[1,128,1024]{2,1,0:T(8,128)(2,1)} %collective-permute-done.6.refs_5_), channel_id=1, source_target_pairs={{0,4},{2,6},{4,0},{6,2},{1,5},{3,7},{5,1},{7,3},{8,12},{10,14},{12... | collective-permute-start | bytes 786440 | tf_op jit(solution)/shard_map/ppermute | solution.py:40
  42.2 8.5 %collective-permute-start.15 = (bf16[1,128,1024]{2,1,0:T(8,128)(2,1)}, bf16[1,128,1024]{2,1,0:T(8,128)(2,1)S(1)}, u32[]{:S(2)}, u32[]{:S(2)}) collective-permute-start(bf16[1,128,1024]{2,1,0:T(8,128)(2,1)} %collective-permute-done.13.refs_12_), channel_id=1, source_target_pairs={{0,4},{2,6},{4,0},{6,2},{1,5},{3,7},{5,1},{7,3},{8,12},{10,14},{12... | collective-permute-start | bytes 786440 | tf_op jit(solution)/shard_map/ppermute | solution.py:40
  42.8 9.7 %collective-permute-start.12 = (bf16[1,128,1024]{2,1,0:T(8,128)(2,1)S(1)}, bf16[1,128,1024]{2,1,0:T(8,128)(2,1)S(1)}, u32[]{:S(2)}, u32[]{:S(2)}) collective-permute-start(bf16[1,128,1024]{2,1,0:T(8,128)(2,1)S(1)} %collective-permute-done.11.refs_10_), channel_id=1, source_target_pairs={{0,2},{2,0},{4,6},{6,4},{1,3},{3,1},{5,7},{7,5},{8,10},{10,8},{12,... | collective-permute-start | bytes 786440 | tf_op jit(solution)/shard_map/ppermute | solution.py:40
  43.6 10.2 %collective-permute-start.16 = (bf16[1,128,1024]{2,1,0:T(8,128)(2,1)S(1)}, bf16[1,128,1024]{2,1,0:T(8,128)(2,1)S(1)}, u32[]{:S(2)}, u32[]{:S(2)}) collective-permute-start(bf16[1,128,1024]{2,1,0:T(8,128)(2,1)S(1)} %collective-permute-done.14.refs_13_), channel_id=1, source_target_pairs={{0,4},{2,6},{4,0},{6,2},{1,5},{3,7},{5,1},{7,3},{8,12},{10,14},{12... | collective-permute-start | bytes 786440 | tf_op jit(solution)/shard_map/ppermute | solution.py:40
  49.2 10.9 %collective-permute-start.25 = (bf16[1,128,1024]{2,1,0:T(8,128)(2,1)S(1)}, bf16[1,128,1024]{2,1,0:T(8,128)(2,1)S(1)}, u32[]{:S(2)}, u32[]{:S(2)}) collective-permute-start(bf16[1,128,1024]{2,1,0:T(8,128)(2,1)S(1)} %collective-permute-done.23.refs_4_), channel_id=1, source_target_pairs={{0,4},{2,6},{4,0},{6,2},{1,5},{3,7},{5,1},{7,3},{8,12},{10,14},{12... | collective-permute-start | bytes 786440 | tf_op jit(solution)/shard_map/ppermute | solution.py:40
  50.4 10.5 %collective-permute-start.22 = (bf16[1,128,1024]{2,1,0:T(8,128)(2,1)}, bf16[1,128,1024]{2,1,0:T(8,128)(2,1)S(1)}, u32[]{:S(2)}, u32[]{:S(2)}) collective-permute-start(bf16[1,128,1024]{2,1,0:T(8,128)(2,1)} %collective-permute-done.21.refs_2_), channel_id=1, source_target_pairs={{0,2},{2,0},{4,6},{6,4},{1,3},{3,1},{5,7},{7,5},{8,10},{10,8},{12,... | collective-permute-start | bytes 786440 | tf_op jit(solution)/shard_map/ppermute | solution.py:40
  50.7 11.5 %collective-permute-start.31 = (bf16[1,128,1024]{2,1,0:T(8,128)(2,1)S(1)}, bf16[1,128,1024]{2,1,0:T(8,128)(2,1)S(1)}, u32[]{:S(2)}, u32[]{:S(2)}) collective-permute-start(bf16[1,128,1024]{2,1,0:T(8,128)(2,1)S(1)} %collective-permute-done.27.refs_8_), channel_id=1, source_target_pairs={{0,8},{8,16},{16,24},{24,0},{1,9},{9,17},{17,25},{25,1},{2,10},{10... | collective-permute-start | bytes 786440 | tf_op jit(solution)/shard_map/ppermute | solution.py:57
  52.6 11.6 %collective-permute-start.29 = (bf16[1,128,1024]{2,1,0:T(8,128)(2,1)S(1)}, bf16[1,128,1024]{2,1,0:T(8,128)(2,1)S(1)}, u32[]{:S(2)}, u32[]{:S(2)}) collective-permute-start(bf16[1,128,1024]{2,1,0:T(8,128)(2,1)S(1)} %collective-permute-done.27.refs_8_), channel_id=1, source_target_pairs={{0,4},{2,6},{4,0},{6,2},{1,5},{3,7},{5,1},{7,3},{8,12},{10,14},{12... | collective-permute-start | bytes 786440 | tf_op jit(solution)/shard_map/ppermute | solution.py:40
  53.8 10.4 %collective-permute-start.28 = (bf16[1,128,1024]{2,1,0:T(8,128)(2,1)S(1)}, bf16[1,128,1024]{2,1,0:T(8,128)(2,1)S(1)}, u32[]{:S(2)}, u32[]{:S(2)}) collective-permute-start(bf16[1,128,1024]{2,1,0:T(8,128)(2,1)S(1)} %collective-permute-done.27.refs_8_), channel_id=1, source_target_pairs={{0,2},{2,0},{4,6},{6,4},{1,3},{3,1},{5,7},{7,5},{8,10},{10,8},{12,... | collective-permute-start | bytes 786440 | tf_op jit(solution)/shard_map/ppermute | solution.py:40
  60.1 17.5 %collective-permute-start.36 = (bf16[2,1024,128]{2,1,0:T(8,128)(2,1)S(1)}, bf16[2,1024,128]{2,1,0:T(8,128)(2,1)S(1)}, u32[]{:S(2)}, u32[]{:S(2)}) collective-permute-start(bf16[2,1024,128]{2,1,0:T(8,128)(2,1)S(1)} %pad_maximum_fusion.refs_3_.refs_5_), channel_id=1, source_target_pairs={{0,8},{8,16},{16,24},{24,0},{1,9},{9,17},{17,25},{25,1},{2,10},{10... | collective-permute-start | bytes 1572872 | tf_op jit(solution)/shard_map/ppermute | solution.py:80
  61.0 19.3 %collective-permute-start.46 = (bf16[2,1024,128]{2,1,0:T(8,128)(2,1)S(1)}, bf16[2,1024,128]{2,1,0:T(8,128)(2,1)S(1)}, u32[]{:S(2)}, u32[]{:S(2)}) collective-permute-start(bf16[2,1024,128]{2,1,0:T(8,128)(2,1)S(1)} %pad_maximum_fusion.refs_3_.refs_5_), channel_id=1, source_target_pairs={{0,2},{2,0},{4,6},{6,4},{1,3},{3,1},{5,7},{7,5},{8,10},{10,8},{12,... | collective-permute-start | bytes 1572872 | tf_op jit(solution)/shard_map/ppermute | solution.py:40
  62.2 16.8 %collective-permute-start.41 = (bf16[2,1024,128]{2,1,0:T(8,128)(2,1)S(1)}, bf16[2,1024,128]{2,1,0:T(8,128)(2,1)S(1)}, u32[]{:S(2)}, u32[]{:S(2)}) collective-permute-start(bf16[2,1024,128]{2,1,0:T(8,128)(2,1)S(1)} %pad_maximum_fusion.1.refs_9_.refs_11_), channel_id=1, source_target_pairs={{0,8},{8,16},{16,24},{24,0},{1,9},{9,17},{17,25},{25,1},{2,10},{10... | collective-permute-start | bytes 1572872 | tf_op jit(solution)/shard_map/ppermute | solution.py:80
  64.2 12.9 %collective-permute-start.26 = (bf16[1,128,1024]{2,1,0:T(8,128)(2,1)S(1)}, bf16[1,128,1024]{2,1,0:T(8,128)(2,1)S(1)}, u32[]{:S(2)}, u32[]{:S(2)}) collective-permute-start(bf16[1,128,1024]{2,1,0:T(8,128)(2,1)S(1)} %collective-permute-done.24.refs_5_), channel_id=1, source_target_pairs={{0,4},{2,6},{4,0},{6,2},{1,5},{3,7},{5,1},{7,3},{8,12},{10,14},{12... | collective-permute-start | bytes 786440 | tf_op jit(solution)/shard_map/ppermute | solution.py:40
  64.2 16.1 %collective-permute-start.32 = (bf16[1,128,1024]{2,1,0:T(8,128)(2,1)S(1)}, bf16[1,128,1024]{2,1,0:T(8,128)(2,1)S(1)}, u32[]{:S(2)}, u32[]{:S(2)}) collective-permute-start(bf16[1,128,1024]{2,1,0:T(8,128)(2,1)S(1)} %collective-permute-done.31.refs_12_), channel_id=1, source_target_pairs={{0,2},{2,0},{4,6},{6,4},{1,3},{3,1},{5,7},{7,5},{8,10},{10,8},{12,... | collective-permute-start | bytes 786440 | tf_op jit(solution)/shard_map/ppermute | solution.py:40
  77.6 9.0 %collective-permute-start.30 = (bf16[1,128,1024]{2,1,0:T(8,128)(2,1)S(1)}, bf16[1,128,1024]{2,1,0:T(8,128)(2,1)S(1)}, u32[]{:S(2)}, u32[]{:S(2)}) collective-permute-start(bf16[1,128,1024]{2,1,0:T(8,128)(2,1)S(1)} %collective-permute-done.29.refs_10_), channel_id=1, source_target_pairs={{0,2},{2,0},{4,6},{6,4},{1,3},{3,1},{5,7},{7,5},{8,10},{10,8},{12,... | collective-permute-start | bytes 786440 | tf_op jit(solution)/shard_map/ppermute | solution.py:40
  79.0 16.5 %collective-permute-start.37 = (bf16[2,1024,128]{2,1,0:T(8,128)(2,1)S(1)}, bf16[2,1024,128]{2,1,0:T(8,128)(2,1)S(1)}, u32[]{:S(2)}, u32[]{:S(2)}) collective-permute-start(bf16[2,1024,128]{2,1,0:T(8,128)(2,1)S(1)} %collective-permute-done.36.refs_5_.refs_7_), channel_id=1, source_target_pairs={{0,8},{8,16},{16,24},{24,0},{1,9},{9,17},{17,25},{25,1},{2,10},{10... | collective-permute-start | bytes 1572872 | tf_op jit(solution)/shard_map/ppermute | solution.py:80
  80.3 20.8 %collective-permute-start.42 = (bf16[2,1024,128]{2,1,0:T(8,128)(2,1)S(1)}, bf16[2,1024,128]{2,1,0:T(8,128)(2,1)S(1)}, u32[]{:S(2)}, u32[]{:S(2)}) collective-permute-start(bf16[2,1024,128]{2,1,0:T(8,128)(2,1)S(1)} %collective-permute-done.41.refs_11_.refs_13_), channel_id=1, source_target_pairs={{0,8},{8,16},{16,24},{24,0},{1,9},{9,17},{17,25},{25,1},{2,10},{10... | collective-permute-start | bytes 1572872 | tf_op jit(solution)/shard_map/ppermute | solution.py:80
  80.4 8.8 %collective-permute-start.34 = (bf16[1,128,1024]{2,1,0:T(8,128)(2,1)S(1)}, bf16[1,128,1024]{2,1,0:T(8,128)(2,1)S(1)}, u32[]{:S(2)}, u32[]{:S(2)}) collective-permute-start(bf16[1,128,1024]{2,1,0:T(8,128)(2,1)S(1)} %collective-permute-done.32.refs_13_), channel_id=1, source_target_pairs={{0,4},{2,6},{4,0},{6,2},{1,5},{3,7},{5,1},{7,3},{8,12},{10,14},{12... | collective-permute-start | bytes 786440 | tf_op jit(solution)/shard_map/ppermute | solution.py:40
  82.8 18.7 %collective-permute-start.17 = (f32[2,2,1024]{2,1,0:T(2,128)S(1)}, f32[2,2,1024]{2,1,0:T(2,128)S(1)}, u32[]{:S(2)}, u32[]{:S(2)}) collective-permute-start(f32[2,2,1024]{2,1,0:T(2,128)S(1)} %pad_maximum_fusion.2), channel_id=1, source_target_pairs={{0,8},{8,16},{16,24},{24,0},{1,9},{9,17},{17,25},{25,1},{2,10},{10... | collective-permute-start | bytes 49160 | tf_op jit(solution)/shard_map/ppermute | solution.py:567
  86.6 15.8 %collective-permute-start.18 = (f32[2,2,1024]{2,1,0:T(2,128)S(1)}, f32[2,2,1024]{2,1,0:T(2,128)S(1)}, u32[]{:S(2)}, u32[]{:S(2)}) collective-permute-start(f32[2,2,1024]{2,1,0:T(2,128)S(1)} %pad_maximum_fusion.2), channel_id=1, source_target_pairs={{0,16},{8,24},{16,0},{24,8},{1,17},{9,25},{17,1},{25,9},{2,18},{10... | collective-permute-start | bytes 49160 | tf_op jit(solution)/shard_map/ppermute | solution.py:567
  89.2 30.9 %collective-permute-start.19 = (f32[2,2,1024]{2,1,0:T(2,128)S(1)}, f32[2,2,1024]{2,1,0:T(2,128)S(1)}, u32[]{:S(2)}, u32[]{:S(2)}) collective-permute-start(f32[2,2,1024]{2,1,0:T(2,128)S(1)} %pad_maximum_fusion.2), channel_id=1, source_target_pairs={{0,24},{8,0},{16,8},{24,16},{1,25},{9,1},{17,9},{25,17},{2,26},{10... | collective-permute-start | bytes 49160 | tf_op jit(solution)/shard_map/ppermute | solution.py:567
  95.6 30.3 %collective-permute-start.49 = (bf16[2,1024,128]{2,1,0:T(8,128)(2,1)S(1)}, bf16[2,1024,128]{2,1,0:T(8,128)(2,1)S(1)}, u32[]{:S(2)}, u32[]{:S(2)}) collective-permute-start(bf16[2,1024,128]{2,1,0:T(8,128)(2,1)S(1)} %pad_maximum_fusion.1.refs_9_.refs_11_), channel_id=1, source_target_pairs={{0,4},{2,6},{4,0},{6,2},{1,5},{3,7},{5,1},{7,3},{8,12},{10,14},{12... | collective-permute-start | bytes 1572872 | tf_op jit(solution)/shard_map/ppermute | solution.py:40
  101.1 24.8 %collective-permute-start.47 = (bf16[2,1024,128]{2,1,0:T(8,128)(2,1)S(1)}, bf16[2,1024,128]{2,1,0:T(8,128)(2,1)S(1)}, u32[]{:S(2)}, u32[]{:S(2)}) collective-permute-start(bf16[2,1024,128]{2,1,0:T(8,128)(2,1)S(1)} %collective-permute-done.36.refs_5_.refs_7_), channel_id=1, source_target_pairs={{0,2},{2,0},{4,6},{6,4},{1,3},{3,1},{5,7},{7,5},{8,10},{10,8},{12,... | collective-permute-start | bytes 1572872 | tf_op jit(solution)/shard_map/ppermute | solution.py:40
  101.5 24.5 %collective-permute-start.50 = (bf16[2,1024,128]{2,1,0:T(8,128)(2,1)S(1)}, bf16[2,1024,128]{2,1,0:T(8,128)(2,1)S(1)}, u32[]{:S(2)}, u32[]{:S(2)}) collective-permute-start(bf16[2,1024,128]{2,1,0:T(8,128)(2,1)S(1)} %collective-permute-done.41.refs_11_.refs_13_), channel_id=1, source_target_pairs={{0,4},{2,6},{4,0},{6,2},{1,5},{3,7},{5,1},{7,3},{8,12},{10,14},{12... | collective-permute-start | bytes 1572872 | tf_op jit(solution)/shard_map/ppermute | solution.py:40
  102.4 23.6 %collective-permute-start.48 = (bf16[2,1024,128]{2,1,0:T(8,128)(2,1)S(1)}, bf16[2,1024,128]{2,1,0:T(8,128)(2,1)S(1)}, u32[]{:S(2)}, u32[]{:S(2)}) collective-permute-start(bf16[2,1024,128]{2,1,0:T(8,128)(2,1)S(1)} %collective-permute-done.37.refs_7_.refs_9_), channel_id=1, source_target_pairs={{0,2},{2,0},{4,6},{6,4},{1,3},{3,1},{5,7},{7,5},{8,10},{10,8},{12,... | collective-permute-start | bytes 1572872 | tf_op jit(solution)/shard_map/ppermute | solution.py:40
  120.1 13.9 %collective-permute-start.51 = (bf16[2,1024,128]{2,1,0:T(8,128)(2,1)S(1)}, bf16[2,1024,128]{2,1,0:T(8,128)(2,1)S(1)}, u32[]{:S(2)}, u32[]{:S(2)}) collective-permute-start(bf16[2,1024,128]{2,1,0:T(8,128)(2,1)S(1)} %collective-permute-done.42.refs_13_.refs_15_), channel_id=1, source_target_pairs={{0,4},{2,6},{4,0},{6,2},{1,5},{3,7},{5,1},{7,3},{8,12},{10,14},{12... | collective-permute-start | bytes 1572872 | tf_op jit(solution)/shard_map/ppermute | solution.py:40
  125.9 19.3 %collective-permute-start.38 = (bf16[2,1024,128]{2,1,0:T(8,128)(2,1)S(1)}, bf16[2,1024,128]{2,1,0:T(8,128)(2,1)S(1)}, u32[]{:S(2)}, u32[]{:S(2)}) collective-permute-start(bf16[2,1024,128]{2,1,0:T(8,128)(2,1)S(1)} %collective-permute-done.37.refs_7_.refs_9_), channel_id=1, source_target_pairs={{0,8},{8,16},{16,24},{24,0},{1,9},{9,17},{17,25},{25,1},{2,10},{10... | collective-permute-start | bytes 1572872 | tf_op jit(solution)/shard_map/ppermute | solution.py:80
  126.0 22.4 %collective-permute-start.43 = (bf16[2,1024,128]{2,1,0:T(8,128)(2,1)S(1)}, bf16[2,1024,128]{2,1,0:T(8,128)(2,1)S(1)}, u32[]{:S(2)}, u32[]{:S(2)}) collective-permute-start(bf16[2,1024,128]{2,1,0:T(8,128)(2,1)S(1)} %collective-permute-done.42.refs_13_.refs_15_), channel_id=1, source_target_pairs={{0,8},{8,16},{16,24},{24,0},{1,9},{9,17},{17,25},{25,1},{2,10},{10... | collective-permute-start | bytes 1572872 | tf_op jit(solution)/shard_map/ppermute | solution.py:80
  136.6 27.2 %collective-permute-start.52 = (bf16[2,192,1536]{2,1,0:T(8,128)(2,1)S(1)}, bf16[2,192,1536]{2,1,0:T(8,128)(2,1)S(1)}, u32[]{:S(2)}, u32[]{:S(2)}) collective-permute-start(bf16[2,192,1536]{2,1,0:T(8,128)(2,1)S(1)} %shard_map.140), channel_id=1, source_target_pairs={{0,1},{1,0},{2,3},{3,2},{4,5},{5,4},{6,7},{7,6},{8,9},{9,8},{10,11... | collective-permute-start | bytes 3538952 | tf_op jit(solution)/shard_map/ppermute | solution.py:580
  145.2 13.4 %collective-permute-start.39 = (bf16[2,1024,128]{2,1,0:T(8,128)(2,1)S(1)}, bf16[2,1024,128]{2,1,0:T(8,128)(2,1)S(1)}, u32[]{:S(2)}, u32[]{:S(2)}) collective-permute-start(bf16[2,1024,128]{2,1,0:T(8,128)(2,1)S(1)} %collective-permute-done.38.refs_3_.refs_5_), channel_id=1, source_target_pairs={{0,2},{2,0},{4,6},{6,4},{1,3},{3,1},{5,7},{7,5},{8,10},{10,8},{12,... | collective-permute-start | bytes 1572872 | tf_op jit(solution)/shard_map/ppermute | solution.py:40
  148.4 10.4 %collective-permute-start.44 = (bf16[2,1024,128]{2,1,0:T(8,128)(2,1)S(1)}, bf16[2,1024,128]{2,1,0:T(8,128)(2,1)S(1)}, u32[]{:S(2)}, u32[]{:S(2)}) collective-permute-start(bf16[2,1024,128]{2,1,0:T(8,128)(2,1)S(1)} %collective-permute-done.43.refs_5_.refs_7_), channel_id=1, source_target_pairs={{0,4},{2,6},{4,0},{6,2},{1,5},{3,7},{5,1},{7,3},{8,12},{10,14},{12... | collective-permute-start | bytes 1572872 | tf_op jit(solution)/shard_map/ppermute | solution.py:40
  159.7 8.1 %collective-permute-start.45 = (bf16[2,192,512]{2,1,0:T(8,128)(2,1)S(1)}, bf16[2,192,512]{2,1,0:T(8,128)(2,1)S(1)}, u32[]{:S(2)}, u32[]{:S(2)}) collective-permute-start(bf16[2,192,512]{2,1,0:T(8,128)(2,1)S(1)} %shard_map.139), channel_id=1, source_target_pairs={{0,1},{1,0},{2,3},{3,2},{4,5},{5,4},{6,7},{7,6},{8,9},{9,8},{10,11... | collective-permute-start | bytes 1179656 | tf_op jit(solution)/shard_map/ppermute | solution.py:581
  (21 other events, 313.1 us)
